TPU v7x, 256 devices: a whole 4x4x8 slice. The times are simulated.
256 devices in a mesh: ep: 64 (over z, y, core), tp: 4 (over x).
Axes of the slice: x: 4, y: 4, z: 8, core: 2. Of those that a mesh axis runs over, the one named last changes fastest.
Arguments:
- query_rows: bfloat16 [8192, 1024], P('ep', 'tp'), may hold values from -10 to 10
- key_rows: bfloat16 [8192, 1024], P('ep', 'tp'), may hold values from -10 to 10
- value_rows: bfloat16 [8192, 1024], P('ep', 'tp'), may hold values from -6 to 6
- key_bias: bfloat16 [8192, 16], P('ep', 'tp'), may hold values from -24 to 4
- mixer_weight: bfloat16 [1024, 2048], P('tp'), may hold values from -0.1875 to 0.1875
- mixer_gain: float32 [2048], replicated, may hold values from 0.1 to 1.9
- routed_input: bfloat16 [24576, 2048], P(('ep', 'tp')), may hold values from -6 to 6
- entry_gain: float32 [2048], replicated, may hold values from 0.1 to 1.9
- expert_index: int32 [24576, 2], P(('ep', 'tp')), may hold values from 0 to 127, all different within a row; in each aligned block of 96 rows (0 to 95, 96 to 191, ...) at most 2 rows name the same one
- route_weights: float32 [24576, 2], P(('ep', 'tp')), may hold values from 0.1 to 1
- expert_gate: bfloat16 [128, 2048, 1024], P('ep', None, 'tp'), may hold values from -0.125 to 0.125
- expert_up: bfloat16 [128, 2048, 1024], P('ep', None, 'tp'), may hold values from -0.125 to 0.125
- expert_down: bfloat16 [128, 1024, 2048], P('ep', 'tp'), may hold values from -0.1875 to 0.1875
- shared_gate: bfloat16 [2048, 1024], P(None, 'tp'), may hold values from -0.125 to 0.125
- shared_up: bfloat16 [2048, 1024], P(None, 'tp'), may hold values from -0.125 to 0.125
- shared_down: bfloat16 [1024, 2048], P('tp'), may hold values from -0.1875 to 0.1875
- exit_gain: float32 [2048], replicated, may hold values from 0.1 to 1.9
Outputs:
- mixer_out: bfloat16 [8192, 2048], P(('ep', 'tp'))
- expert_out: bfloat16 [24576, 2048], P(('ep', 'tp'))
Inputs may be any that keep to these rules, and one draw needn't show every extreme that they name: `expert_index`: in each aligned block of 96 rows (the rows of one device) no expert is named by more than 2 rows, a bound that some block reaches; each row names 2 different experts.
All inputs are finite; a program needn't handle non-finite values.
Results may differ from a plain program's by a relative error of at most 0.012.
Values may be sent and summed in bfloat16 or wider, within the bound.
A program may use at most 128 MiB of HBM per device.

v0:
```python
import jax
import jax.numpy as jnp
from jax import lax
from jax.sharding import PartitionSpec as P

EPS = 1e-06


def in_one_piece(arrays, axis, dim, along):
    widths = [a.shape[along] for a in arrays]
    both = jnp.concatenate(arrays, axis=along)
    filled = lax.all_gather(both, axis, axis=dim, tiled=True)
    return tuple(jnp.split(filled, [sum(widths[:k]) for k in range(1, len(widths))], axis=along))


def in_blocks(array, dim, peers):
    before, after = (array.shape[:dim], array.shape[dim + 1 :])
    return jnp.moveaxis(array.reshape(*before, peers, -1, *after), dim, 0)


def sum_at_owner(array, axis, dim):
    peers = lax.axis_size(axis)
    tiles = lax.all_to_all(in_blocks(array, dim, peers), axis, 0, 0, tiled=True)
    return jnp.sum(tiles.astype(jnp.float32), axis=0)


def root_norm(values, gain_row):
    return values * lax.rsqrt(jnp.mean(values * values, axis=-1, keepdims=True) + EPS) * gain_row


def rounded_term(partial_value):
    return lax.optimization_barrier(partial_value.astype(jnp.bfloat16)).astype(jnp.float32)


def block_shards(shard_rows, ep_size):
    shards = 1
    while shards * shard_rows < 512 and ep_size % (2 * shards) == 0:
        shards = shards * 2
    return shards


def break_scores(query_split, block_keys, block_bias, query_pos, key_start):
    head_count = query_split.shape[1]
    key_count = block_keys.shape[0]
    keys_split = block_keys.reshape(key_count, head_count, query_split.shape[2])
    scores = jnp.einsum("qhd,khd->hqk", query_split, keys_split, preferred_element_type=jnp.float32)
    scores = (
        scores * query_split.shape[2] ** (-0.5)
        + jnp.transpose(block_bias.astype(jnp.float32))[:, None, :]
    )
    key_pos = key_start + jnp.arange(key_count, dtype=jnp.int32)
    causal = (key_pos[None, :] < query_pos[:, None])[None]
    fail_logs = jnp.where(causal, -jax.nn.softplus(scores), 0.0)
    return (scores, fail_logs, causal)


def break_values(scores, fail_logs, causal, offset, block_values):
    later_sum = lax.cumsum(fail_logs, axis=2, reverse=True) - fail_logs + offset[:, :, None]
    weights = jnp.where(causal, jnp.exp(jax.nn.log_sigmoid(scores) + later_sum), 0.0).astype(
        jnp.bfloat16
    )
    values_split = block_values.reshape(block_values.shape[0], scores.shape[0], -1)
    return jnp.einsum("hqk,khd->qhd", weights, values_split, preferred_element_type=jnp.float32)


def shared_term_of(own_all, shared_gate, shared_up, shared_down):
    gate_part = jnp.dot(own_all, shared_gate, preferred_element_type=jnp.float32)
    up_part = jnp.dot(own_all, shared_up, preferred_element_type=jnp.float32)
    hidden = (jax.nn.silu(gate_part) * up_part).astype(jnp.bfloat16)
    return rounded_term(jnp.dot(hidden, shared_down, preferred_element_type=jnp.float32))


def on_device(
    query_rows,
    key_rows,
    value_rows,
    key_bias,
    mixer_weight,
    mixer_gain,
    routed_input,
    entry_gain,
    expert_index,
    route_weights,
    expert_gate,
    expert_up,
    expert_down,
    shared_gate,
    shared_up,
    shared_down,
    exit_gain,
):
    shard_rows = query_rows.shape[0]
    head_count = key_bias.shape[1]
    head_size = query_rows.shape[1] // head_count
    ep_size = lax.axis_size("ep")
    tp_size = lax.axis_size("tp")
    own_index = lax.axis_index("ep")
    query_split = query_rows.reshape(shard_rows, head_count, head_size)
    query_pos = own_index * shard_rows + jnp.arange(shard_rows, dtype=jnp.int32)
    span_shards = block_shards(shard_rows, ep_size)
    empty_output = jnp.zeros((shard_rows, head_count, head_size), jnp.float32)
    all_keys, all_values, all_bias = in_one_piece((key_rows, value_rows, key_bias), "ep", 0, 1)
    block_rows = span_shards * shard_rows
    own_block = own_index * shard_rows // block_rows

    def backward_turn(turn_index, carried_pair):
        output, carried = carried_pair
        block_start = (own_block - turn_index) * block_rows
        block_keys = lax.dynamic_slice_in_dim(all_keys, block_start, block_rows, 0)
        block_values = lax.dynamic_slice_in_dim(all_values, block_start, block_rows, 0)
        block_bias = lax.dynamic_slice_in_dim(all_bias, block_start, block_rows, 0)
        scores, fail_logs, causal = break_scores(
            query_split, block_keys, block_bias, query_pos, block_start
        )
        output = output + break_values(scores, fail_logs, causal, carried, block_values)
        return (output, carried + jnp.sum(fail_logs, axis=2))

    carried_zero = jnp.zeros((head_count, shard_rows), jnp.float32)
    output, unused = lax.fori_loop(0, own_block + 1, backward_turn, (empty_output, carried_zero))
    attended = output.reshape(shard_rows, head_count * head_size).astype(jnp.bfloat16)
    mixer_term = rounded_term(jnp.dot(attended, mixer_weight, preferred_element_type=jnp.float32))
    row_count = routed_input.shape[0]
    top_count = expert_index.shape[1]
    local_experts = expert_gate.shape[0]
    model_width = routed_input.shape[1]
    expert_count = local_experts * ep_size
    capacity = 3 * row_count * top_count // (2 * expert_count)
    slot_total = expert_count * capacity
    normed = root_norm(routed_input.astype(jnp.float32), entry_gain).astype(jnp.bfloat16)
    flat_expert = expert_index.reshape(-1)
    onehot = (flat_expert[:, None] == jnp.arange(expert_count, dtype=jnp.int32)[None, :]).astype(
        jnp.int32
    )
    slot_rank = jnp.sum((jnp.cumsum(onehot, axis=0) - onehot) * onehot, axis=1)
    slot_index = (flat_expert * capacity + slot_rank).reshape(row_count, top_count)
    matches = slot_index[None, :, :] == jnp.arange(slot_total, dtype=jnp.int32)[:, None, None]
    selector = jnp.any(matches, axis=2).astype(jnp.bfloat16)
    outgoing = jnp.dot(selector, normed, preferred_element_type=jnp.float32).astype(jnp.bfloat16)
    outgoing = outgoing.reshape(expert_count, capacity, model_width)
    arrived = lax.all_to_all(outgoing, "ep", split_axis=0, concat_axis=0, tiled=True)
    routed_all, own_all = (
        lax.all_gather(arrived.reshape(slot_total, model_width), "tp", axis=0, tiled=True),
        lax.all_gather(normed, "tp", axis=0, tiled=True),
    )
    routed_split = routed_all.reshape(tp_size, ep_size, local_experts, capacity, model_width)
    gate_part = jnp.einsum(
        "tsecd,edf->tsecf", routed_split, expert_gate, preferred_element_type=jnp.float32
    )
    up_part = jnp.einsum(
        "tsecd,edf->tsecf", routed_split, expert_up, preferred_element_type=jnp.float32
    )
    hidden = (jax.nn.silu(gate_part) * up_part).astype(jnp.bfloat16)
    routed_term = jnp.einsum(
        "tsecf,efd->tsecd", hidden, expert_down, preferred_element_type=jnp.float32
    )
    routed_term = rounded_term(routed_term.reshape(tp_size * slot_total, model_width))
    shared_term = shared_term_of(own_all, shared_gate, shared_up, shared_down)
    mixer_sum, routed_sum, shared_sum = (
        sum_at_owner(mixer_term.astype(jnp.bfloat16), "tp", 0),
        sum_at_owner(routed_term.astype(jnp.bfloat16), "tp", 0),
        sum_at_owner(shared_term.astype(jnp.bfloat16), "tp", 0),
    )
    returned_rows = routed_sum.astype(jnp.bfloat16).reshape(expert_count, capacity, model_width)
    back_rows = lax.all_to_all(
        returned_rows, "ep", split_axis=0, concat_axis=0, tiled=True
    ).reshape(slot_total, model_width)
    gathered = back_rows[slot_index].astype(jnp.float32)
    routed = jnp.sum(route_weights[:, :, None] * gathered, axis=1)
    combined = routed + shared_sum
    expert_out = root_norm(combined, exit_gain).astype(jnp.bfloat16)
    mixer_out = root_norm(mixer_sum, mixer_gain).astype(jnp.bfloat16)
    return (mixer_out, expert_out)


def solution(mesh):
    in_specs = (
        P("ep", "tp"),
        P("ep", "tp"),
        P("ep", "tp"),
        P("ep", "tp"),
        P("tp", None),
        P(),
        P(("ep", "tp"), None),
        P(),
        P(("ep", "tp"), None),
        P(("ep", "tp"), None),
        P("ep", None, "tp"),
        P("ep", None, "tp"),
        P("ep", "tp", None),
        P(None, "tp"),
        P(None, "tp"),
        P("tp", None),
        P(),
    )
    out_specs = (P(("ep", "tp"), None), P(("ep", "tp"), None))
    return jax.shard_map(
        on_device, mesh=mesh, in_specs=in_specs, out_specs=out_specs, check_vma=False
    )
```

profile of v0, /device:TPU:248, one launch (start us, length us, event | category | flops | bytes accessed | tf_op | source)
XLA Modules:
  0.0 446.4 jit_solution(14355067020275289579)
XLA Ops:
  14.1 1.5 reshape.136
  15.6 34.0 %all_to_all.25 = bf16[128,2,2048]{2,1,0:T(2,128)(2,1)S(1)} all-to-all(bf16[128,2,2048]{2,1,0:T(2,128)(2,1)} %reshape.136), channel_id=1, replica_groups=mesh['ep'=64,'tp'=4] {'ep'}, dimensions={0} | all-to-all | bytes 2097152 | tf_op jit(solution)/shard_map/all_to_all | solution.py:140
  54.3 48.0 %all-gather.6.cloned.1.call-done = bf16[1024,2048]{1,0:T(8,128)(2,1)} async-done(((bf16[256,2048]{1,0:T(8,128)(2,1)}), bf16[1024,2048]{1,0:T(8,128)(2,1)}) %all-gather.6.cloned.1.call-update) | async-done | bytes 4194320 | tf_op jit(solution)/shard_map/all_gather | solution.py:142
  102.3 7.8 %reshape.138 = bf16[4,64,2,2,2048]{4,3,2,1,0:T(2,128)(2,1)} reshape(bf16[1024,2048]{1,0:T(8,128)(2,1)} %all-gather.6.cloned.1.call-done) | data formatting | bytes 8388608 | tf_op jit(solution)/shard_map/reshape | solution.py:145
  110.1 7.4 %fusion.23 = f32[4,64,2,2,256]{4,1,3,0,2:T(8,128)S(1)} fusion(bf16[2,2048,256]{2,1,0:T(8,128)(2,1)} %param.29, bf16[4,64,2,2,2048]{4,3,2,1,0:T(2,128)(2,1)} %reshape.138), kind=kOutput, calls=%fused_computation.42 | convolution fusion | flops 1073741824 | bytes 7340032 | tf_op jit(solution)/shard_map/tsecd,edf->tsecf/dot_general | solution.py:146
  117.6 10.8 %convert_bitcast_fusion.1 = bf16[4,64,2,2,2048]{4,1,3,0,2:T(8,128)(2,1)} fusion(bf16[2,256,2048]{2,1,0:T(8,128)(2,1)S(1)} %copy-done, bf16[2,2048,256]{2,1,0:T(8,128)(2,1)} %param.30, bf16[4,64,2,2,2048]{4,3,2,1,0:T(2,128)(2,1)} %reshape.138, f32[4,64,2,2,256]{4,1,3,0,2:T(8,128)S(1)} %fusion.23), kind=kOutput, calls=%fused_computation.29 | convolution fusion | flops 2151153664 | bytes 13631488 | tf_op jit(solution)/shard_map/tsecf,efd->tsecd/dot_general | solution.py:153
  128.4 8.8 %copy.70 = bf16[4,64,2,2,2048]{4,3,2,1,0:T(2,128)(2,1)} copy(bf16[4,64,2,2,2048]{4,1,3,0,2:T(8,128)(2,1)} %convert_bitcast_fusion.1) | data formatting | bytes 8388608 | tf_op jit(solution)/shard_map/convert_element_type | solution.py:32
  137.2 7.2 %convert_element_type.80 = bf16[1024,2048]{1,0:T(8,128)(2,1)} reshape(bf16[4,64,2,2,2048]{4,3,2,1,0:T(2,128)(2,1)} %copy.70) | data formatting | bytes 8388608 | tf_op jit(solution)/shard_map/convert_element_type | solution.py:32
  144.4 5.0 %all-to-all-start.2 = ((bf16[4,256,2048]{2,1,0:T(8,128)(2,1)}), bf16[4,256,2048]{2,1,0:T(8,128)(2,1)}, u32[]{:S(2)}, u32[]{:S(2)}) async-start(bf16[4,256,2048]{2,1,0:T(8,128)(2,1)} %bitcast.107), calls=%async_computation.2 | async-start | bytes 8388608 | tf_op jit(solution)/shard_map/all_to_all | solution.py:23
  149.5 2.1 fusion.69
  151.6 4.5 %convolution_convert_fusion = bf16[384,2048]{1,0:T(8,128)(2,1)} fusion(bf16[256,2048]{1,0:T(8,128)(2,1)} %param.34, bf16[384,2048]{1,0:T(8,128)(2,1)S(1)} %copy-done.10, bf16[2048,256]{1,0:T(8,128)(2,1)} %param.33, f32[384,256]{1,0:T(8,128)S(1)} %fusion.69), kind=kOutput, calls=%fused_computation.35 | convolution fusion | flops 806682624 | bytes 5636096 | tf_op jit(solution)/shard_map/dot_general | solution.py:70
  156.1 42.3 %all-to-all-done.2 = bf16[4,256,2048]{2,1,0:T(8,128)(2,1)} async-done(((bf16[4,256,2048]{2,1,0:T(8,128)(2,1)}), bf16[4,256,2048]{2,1,0:T(8,128)(2,1)}, u32[]{:S(2)}, u32[]{:S(2)}) %all-to-all-start.2) | async-done | bytes 4194336 | tf_op jit(solution)/shard_map/all_to_all | solution.py:23
  198.4 3.6 all-to-all-start.4
  202.0 3.1 reduce_sum.91
  205.2 1.5 reshape.140
  206.7 15.2 %all-to-all-done.4 = bf16[4,96,2048]{2,1,0:T(8,128)(2,1)S(1)} async-done(((bf16[4,96,2048]{2,1,0:T(8,128)(2,1)}), bf16[4,96,2048]{2,1,0:T(8,128)(2,1)S(1)}, u32[]{:S(2)}, u32[]{:S(2)}) %all-to-all-start.4) | async-done | bytes 1572896 | tf_op jit(solution)/shard_map/all_to_all | solution.py:23
  222.0 10.6 %all-to-all-start.3 = ((bf16[128,2,2048]{2,1,0:T(2,128)(2,1)}), bf16[128,2,2048]{2,1,0:T(2,128)(2,1)S(1)}, u32[]{:S(2)}, u32[]{:S(2)}) async-start(bf16[128,2,2048]{2,1,0:T(2,128)(2,1)} %reshape.140), calls=%async_computation.3 | async-start | bytes 2097152 | tf_op jit(solution)/shard_map/all_to_all | solution.py:164
  234.2 23.3 %all-to-all-done.3 = bf16[128,2,2048]{2,1,0:T(2,128)(2,1)S(1)} async-done(((bf16[128,2,2048]{2,1,0:T(2,128)(2,1)}), bf16[128,2,2048]{2,1,0:T(2,128)(2,1)S(1)}, u32[]{:S(2)}, u32[]{:S(2)}) %all-to-all-start.3) | async-done | bytes 1048608 | tf_op jit(solution)/shard_map/all_to_all | solution.py:164
  257.9 2.1 gather_fusion
  260.0 2.2 reshape.154
  262.2 2.3 multiply_reduce_fusion
  265.7 5.9 %fusion.68 = (bf16[8192,256]{0,1:T(8,128)(2,1)}, bf16[8192,256]{0,1:T(8,128)(2,1)}) fusion(bf16[8192,516]{0,1:T(8,128)(2,1)} %all-gather.4.cloned.1.call-done), kind=kLoop, calls=%fused_computation.89 | loop fusion | bytes 16777216 | tf_op jit(solution)/shard_map/split | solution.py:13
  271.6 150.8 %while.13 = (s32[]{:T(128)}, f32[128,4,64]{0,2,1:T(8,128)S(1)}, f32[4,128]{1,0:T(4,128)S(1)}, s32[]{:T(128)}, s32[]{:T(128)}, /*index=5*/bf16[8192,256]{0,1:T(8,...) while((s32[]{:T(128)}, f32[128,4,64]{0,2,1:T(8,128)S(1)}, ...), condition=%wide.region_4.5_spmd.clone, body=%wide.region_0.4_spmd.clone.sunk | while | flops 109160584 | bytes 13726939 | solution.py:119
  274.1 4.8 %fusion.98 = f32[4,128,4,128]{1,2,3,0:T(4,128)S(1)} fusion(f32[4,128,4,128]{1,3,2,0:T(8,128)S(1)} %bitcast.105), kind=kOutput, calls=%fused_computation.18.clone.1 | output fusion | flops 33292288 | bytes 2097152 | tf_op jit(solution)/shard_map/reduce-window
  279.3 1.5 fusion.99
  283.5 4.8 %fusion.98 = f32[4,128,4,128]{1,2,3,0:T(4,128)S(1)} fusion(f32[4,128,4,128]{1,3,2,0:T(8,128)S(1)} %bitcast.105), kind=kOutput, calls=%fused_computation.18.clone.1 | output fusion | flops 33292288 | bytes 2097152 | tf_op jit(solution)/shard_map/reduce-window
  288.7 1.5 fusion.99
  293.0 4.8 %fusion.98 = f32[4,128,4,128]{1,2,3,0:T(4,128)S(1)} fusion(f32[4,128,4,128]{1,3,2,0:T(8,128)S(1)} %bitcast.105), kind=kOutput, calls=%fused_computation.18.clone.1 | output fusion | flops 33292288 | bytes 2097152 | tf_op jit(solution)/shard_map/reduce-window
  302.4 4.8 %fusion.98 = f32[4,128,4,128]{1,2,3,0:T(4,128)S(1)} fusion(f32[4,128,4,128]{1,3,2,0:T(8,128)S(1)} %bitcast.105), kind=kOutput, calls=%fused_computation.18.clone.1 | output fusion | flops 33292288 | bytes 2097152 | tf_op jit(solution)/shard_map/reduce-window
  311.8 4.8 %fusion.98 = f32[4,128,4,128]{1,2,3,0:T(4,128)S(1)} fusion(f32[4,128,4,128]{1,3,2,0:T(8,128)S(1)} %bitcast.105), kind=kOutput, calls=%fused_computation.18.clone.1 | output fusion | flops 33292288 | bytes 2097152 | tf_op jit(solution)/shard_map/reduce-window
  321.2 4.8 %fusion.98 = f32[4,128,4,128]{1,2,3,0:T(4,128)S(1)} fusion(f32[4,128,4,128]{1,3,2,0:T(8,128)S(1)} %bitcast.105), kind=kOutput, calls=%fused_computation.18.clone.1 | output fusion | flops 33292288 | bytes 2097152 | tf_op jit(solution)/shard_map/reduce-window
  326.4 1.5 fusion.99
  330.7 4.8 %fusion.98 = f32[4,128,4,128]{1,2,3,0:T(4,128)S(1)} fusion(f32[4,128,4,128]{1,3,2,0:T(8,128)S(1)} %bitcast.105), kind=kOutput, calls=%fused_computation.18.clone.1 | output fusion | flops 33292288 | bytes 2097152 | tf_op jit(solution)/shard_map/reduce-window
  335.8 1.5 fusion.99
  340.1 4.8 %fusion.98 = f32[4,128,4,128]{1,2,3,0:T(4,128)S(1)} fusion(f32[4,128,4,128]{1,3,2,0:T(8,128)S(1)} %bitcast.105), kind=kOutput, calls=%fused_computation.18.clone.1 | output fusion | flops 33292288 | bytes 2097152 | tf_op jit(solution)/shard_map/reduce-window
  349.5 4.8 %fusion.98 = f32[4,128,4,128]{1,2,3,0:T(4,128)S(1)} fusion(f32[4,128,4,128]{1,3,2,0:T(8,128)S(1)} %bitcast.105), kind=kOutput, calls=%fused_computation.18.clone.1 | output fusion | flops 33292288 | bytes 2097152 | tf_op jit(solution)/shard_map/reduce-window
  358.9 4.8 %fusion.98 = f32[4,128,4,128]{1,2,3,0:T(4,128)S(1)} fusion(f32[4,128,4,128]{1,3,2,0:T(8,128)S(1)} %bitcast.105), kind=kOutput, calls=%fused_computation.18.clone.1 | output fusion | flops 33292288 | bytes 2097152 | tf_op jit(solution)/shard_map/reduce-window
  368.4 4.8 %fusion.98 = f32[4,128,4,128]{1,2,3,0:T(4,128)S(1)} fusion(f32[4,128,4,128]{1,3,2,0:T(8,128)S(1)} %bitcast.105), kind=kOutput, calls=%fused_computation.18.clone.1 | output fusion | flops 33292288 | bytes 2097152 | tf_op jit(solution)/shard_map/reduce-window
  377.8 4.8 %fusion.98 = f32[4,128,4,128]{1,2,3,0:T(4,128)S(1)} fusion(f32[4,128,4,128]{1,3,2,0:T(8,128)S(1)} %bitcast.105), kind=kOutput, calls=%fused_computation.18.clone.1 | output fusion | flops 33292288 | bytes 2097152 | tf_op jit(solution)/shard_map/reduce-window
  387.2 4.8 %fusion.98 = f32[4,128,4,128]{1,2,3,0:T(4,128)S(1)} fusion(f32[4,128,4,128]{1,3,2,0:T(8,128)S(1)} %bitcast.105), kind=kOutput, calls=%fused_computation.18.clone.1 | output fusion | flops 33292288 | bytes 2097152 | tf_op jit(solution)/shard_map/reduce-window
  396.6 4.8 %fusion.98 = f32[4,128,4,128]{1,2,3,0:T(4,128)S(1)} fusion(f32[4,128,4,128]{1,3,2,0:T(8,128)S(1)} %bitcast.105), kind=kOutput, calls=%fused_computation.18.clone.1 | output fusion | flops 33292288 | bytes 2097152 | tf_op jit(solution)/shard_map/reduce-window
  406.0 4.8 %fusion.98 = f32[4,128,4,128]{1,2,3,0:T(4,128)S(1)} fusion(f32[4,128,4,128]{1,3,2,0:T(8,128)S(1)} %bitcast.105), kind=kOutput, calls=%fused_computation.18.clone.1 | output fusion | flops 33292288 | bytes 2097152 | tf_op jit(solution)/shard_map/reduce-window
  411.2 1.5 fusion.99
  415.5 4.8 %fusion.98 = f32[4,128,4,128]{1,2,3,0:T(4,128)S(1)} fusion(f32[4,128,4,128]{1,3,2,0:T(8,128)S(1)} %bitcast.105), kind=kOutput, calls=%fused_computation.18.clone.1 | output fusion | flops 33292288 | bytes 2097152 | tf_op jit(solution)/shard_map/reduce-window
  420.6 1.5 fusion.99
  422.5 2.5 convolution_convert_fusion.2
  425.0 3.5 all-to-all-start
  429.3 9.1 %all-to-all-done = bf16[4,32,2048]{2,1,0:T(8,128)(2,1)S(1)} async-done(((bf16[4,32,2048]{2,1,0:T(8,128)(2,1)}), bf16[4,32,2048]{2,1,0:T(8,128)(2,1)S(1)}, u32[]{:S(2)}, u32[]{:S(2)}) %all-to-all-start) | async-done | bytes 524320 | tf_op jit(solution)/shard_map/all_to_all | solution.py:23
  (293 shorter events, 79.8 us)
Async XLA Ops:
  7.2 110.4 %copy-start = (bf16[2,256,2048]{2,1,0:T(8,128)(2,1)S(1)}, bf16[2,256,2048]{2,1,0:T(8,128)(2,1)}, u32[]{:S(2)}) copy-start(bf16[2,256,2048]{2,1,0:T(8,128)(2,1)} %param.31) | copy-start | bytes 6291460
  7.2 95.1 %all-gather.6.cloned.1.call-start = ((), (), s32[]{:S(2)}) async-start(), calls=%async_computation.6 | async-start | bytes 5242880 | tf_op jit(solution)/shard_map/all_gather | solution.py:142
  12.8 36.8 %copy-start.2 = (bf16[96,2048]{1,0:T(8,128)(2,1)}, bf16[96,2048]{1,0:T(8,128)(2,1)S(1)}, u32[]{:S(2)}) copy-start(bf16[96,2048]{1,0:T(8,128)(2,1)S(1)} %fusion.53) | copy-start | bytes 1179652
  49.6 4.0 copy-start.8
  50.9 98.6 %all-gather.8.cloned.1.call-start = ((), (), s32[]{:S(2)}) async-start(), calls=%async_computation.7 | async-start | bytes 1966080 | tf_op jit(solution)/shard_map/all_gather | solution.py:143
  51.6 214.0 %all-gather.4.cloned.1.call-start = ((), (), s32[]{:S(2)}) async-start(), calls=%async_computation.5 | async-start | bytes 8652800 | tf_op jit(solution)/shard_map/all_gather | solution.py:12
  144.4 5.1 %copy-start.11 = (bf16[2048,256]{1,0:T(8,128)(2,1)S(1)}, bf16[2048,256]{1,0:T(8,128)(2,1)}, u32[]{:S(2)}) copy-start(bf16[2048,256]{1,0:T(8,128)(2,1)} %param.32) | copy-start | bytes 3145732
  144.4 54.0 %all-to-all-start.2 = ((bf16[4,256,2048]{2,1,0:T(8,128)(2,1)}), bf16[4,256,2048]{2,1,0:T(8,128)(2,1)}, u32[]{:S(2)}, u32[]{:S(2)}) async-start(bf16[4,256,2048]{2,1,0:T(8,128)(2,1)} %bitcast.107), calls=%async_computation.2 | async-start | bytes 8388608 | tf_op jit(solution)/shard_map/all_to_all | solution.py:23
  149.5 2.1 copy-start.10
  198.4 23.5 %all-to-all-start.4 = ((bf16[4,96,2048]{2,1,0:T(8,128)(2,1)}), bf16[4,96,2048]{2,1,0:T(8,128)(2,1)S(1)}, u32[]{:S(2)}, u32[]{:S(2)}) async-start(bf16[4,96,2048]{2,1,0:T(8,128)(2,1)} %bitcast.109), calls=%async_computation.4 | async-start | bytes 3145728 | tf_op jit(solution)/shard_map/all_to_all | solution.py:23
  205.2 27.4 %copy-start.5 = (bf16[128,256]{1,0:T(8,128)(2,1)S(1)}, bf16[128,256]{1,0:T(8,128)(2,1)}, u32[]{:S(2)}) copy-start(bf16[128,256]{1,0:T(8,128)(2,1)} %param.19) | copy-start | bytes 196612
  205.2 27.8 %copy-start.9 = (f32[96,2]{0,1:T(2,128)S(1)}, f32[96,2]{0,1:T(2,128)}, u32[]{:S(2)}) copy-start(f32[96,2]{0,1:T(2,128)} %param.28) | copy-start | bytes 2308
  222.0 35.5 %all-to-all-start.3 = ((bf16[128,2,2048]{2,1,0:T(2,128)(2,1)}), bf16[128,2,2048]{2,1,0:T(2,128)(2,1)S(1)}, u32[]{:S(2)}, u32[]{:S(2)}) async-start(bf16[128,2,2048]{2,1,0:T(2,128)(2,1)} %reshape.140), calls=%async_computation.3 | async-start | bytes 2097152 | tf_op jit(solution)/shard_map/all_to_all | solution.py:164
  260.0 4.5 %copy-start.4 = (f32[96,2048]{1,0:T(8,128)S(1)}, f32[96,2048]{1,0:T(8,128)}, u32[]{:S(2)}) copy-start(f32[96,2048]{1,0:T(8,128)} %convert_reduce_fusion) | copy-start | bytes 2359300
  265.7 5.9 %slice-start = ((bf16[8192,516]{0,1:T(8,128)(2,1)}), bf16[8192,4]{0,1:T(4,128)(2,1)S(1)}, s32[]{:S(2)}) async-start(bf16[8192,516]{0,1:T(8,128)(2,1)} %all-gather.4.cloned.1.call-done), calls=%async_computation.8 | async-start | bytes 131072 | tf_op jit(solution)/shard_map/split | solution.py:13
  422.4 6.0 %copy-start.3 = (f32[96,2048]{1,0:T(8,128)S(1)}, f32[96,2048]{1,0:T(8,128)}, u32[]{:S(2)}) copy-start(f32[96,2048]{1,0:T(8,128)} %get-tuple-element.101) | copy-start | bytes 2359300
  422.4 6.0 %copy-start.6 = (f32[2048]{0:T(1024)S(1)}, f32[2048]{0:T(1024)}, u32[]{:S(2)}) copy-start(f32[2048]{0:T(1024)} %param.35) | copy-start | bytes 24580
  422.4 16.2 %copy-start.7 = (f32[2048]{0:T(1024)S(1)}, f32[2048]{0:T(1024)}, u32[]{:S(2)}) copy-start(f32[2048]{0:T(1024)} %param.24) | copy-start | bytes 24580
  422.4 17.0 %copy-start.1 = (bf16[2,256,2048]{2,1,0:T(8,128)(2,1)S(1)}, bf16[2,256,2048]{2,1,0:T(8,128)(2,1)}, u32[]{:S(2)}) copy-start(bf16[2,256,2048]{2,1,0:T(8,128)(2,1)} %param.31) | copy-start | bytes 6291460
  425.0 13.5 %all-to-all-start = ((bf16[4,32,2048]{2,1,0:T(8,128)(2,1)}), bf16[4,32,2048]{2,1,0:T(8,128)(2,1)S(1)}, u32[]{:S(2)}, u32[]{:S(2)}) async-start(bf16[4,32,2048]{2,1,0:T(8,128)(2,1)} %bitcast.2), calls=%async_computation | async-start | bytes 1048576 | tf_op jit(solution)/shard_map/all_to_all | solution.py:23
Sparse Core Ops, SparseCore 0:
  51.0 51.2 all-gather.5
  104.7 29.3 all-gather.7
  136.7 85.6 all-gather.3
where the time goes:
time: 451 us; the launch traced here: 446 us
  waiting for transfers between devices  139 us (31%)
  other arithmetic  121 us (27%)
  local copies, waits for them, and re-layouts  61.6 us (14%)
  matrix products  51.7 us (11%)
  blocking collectives  34 us (8%)
  starting transfers between devices  22.8 us (5%)
  between operations  14.6 us (3%)
    another operation x36, other arithmetic  77.5 us
    all_to_all x3, waiting for transfers between devices, sum_at_owner(): tiles = lax.all_to_all(in_blocks(array, dim, peers), axis, 0, 0, tiled=True)  66.7 us
    all_gather x1, waiting for transfers between devices, on_device(): lax.all_gather(arrived.reshape(slot_total, model_width), 'tp', axis=0, ti...  48 us
    all_to_all x1, blocking collectives, on_device(): lax.all_to_all(outgoing, 'ep', split_axis=0, concat_axis=0, tiled=True)  34 us
    convert_element_type x16, other arithmetic, break_values(): jnp.where(causal, jnp.exp(jax.nn.log_sigmoid(scores) + later_sum), 0.0)  23.7 us
    all_to_all x1, waiting for transfers between devices, on_device(): lax.all_to_all(returned_rows, 'ep', split_axis=0, concat_axis=0, tiled=True)  23.3 us
    dot_general x16, matrix products, break_scores(): jnp.einsum('qhd,khd->hqk', query_split, keys_split, preferred_element_typ...  19.5 us
    dynamic_slice x16, local copies, waits for them, and re-layouts, backward_turn(): block_keys = lax.dynamic_slice_in_dim(all_keys, block_start, block_rows, 0)  17.1 us
  transfers between devices with their start and end apart: 7, of which 5 were waited for; matrix products, arithmetic and copies ran while one was open for 15% of the time, Pallas kernels for 0%

commit v1 on v0

--- a/solution.py
+++ b/solution.py
@@ -1,6 +1,8 @@
 import jax
 import jax.numpy as jnp
 from jax import lax
+from jax.experimental import pallas as pl
+from jax.experimental.pallas import tpu as pltpu
 from jax.sharding import PartitionSpec as P
 
 EPS = 1e-06
@@ -32,35 +34,94 @@
     return lax.optimization_barrier(partial_value.astype(jnp.bfloat16)).astype(jnp.float32)
 
 
-def block_shards(shard_rows, ep_size):
-    shards = 1
-    while shards * shard_rows < 512 and ep_size % (2 * shards) == 0:
-        shards = shards * 2
-    return shards
-
-
-def break_scores(query_split, block_keys, block_bias, query_pos, key_start):
-    head_count = query_split.shape[1]
-    key_count = block_keys.shape[0]
-    keys_split = block_keys.reshape(key_count, head_count, query_split.shape[2])
-    scores = jnp.einsum("qhd,khd->hqk", query_split, keys_split, preferred_element_type=jnp.float32)
-    scores = (
-        scores * query_split.shape[2] ** (-0.5)
-        + jnp.transpose(block_bias.astype(jnp.float32))[:, None, :]
-    )
-    key_pos = key_start + jnp.arange(key_count, dtype=jnp.int32)
-    causal = (key_pos[None, :] < query_pos[:, None])[None]
-    fail_logs = jnp.where(causal, -jax.nn.softplus(scores), 0.0)
-    return (scores, fail_logs, causal)
-
-
-def break_values(scores, fail_logs, causal, offset, block_values):
-    later_sum = lax.cumsum(fail_logs, axis=2, reverse=True) - fail_logs + offset[:, :, None]
-    weights = jnp.where(causal, jnp.exp(jax.nn.log_sigmoid(scores) + later_sum), 0.0).astype(
-        jnp.bfloat16
-    )
-    values_split = block_values.reshape(block_values.shape[0], scores.shape[0], -1)
-    return jnp.einsum("hqk,khd->qhd", weights, values_split, preferred_element_type=jnp.float32)
+LOG2E = 1.4426950408889634
+
+
+def stick_block(query, block_keys, block_values, bias, carry, tri, mask):
+    scores = lax.dot_general(query, block_keys, (((1,), (1,)), ((), ())), preferred_element_type=jnp.float32)
+    level = (scores + bias) * LOG2E
+    fail = jnp.maximum(level, 0.0) + jnp.log2(1.0 + jnp.exp2(-jnp.abs(level)))
+    if mask is not None:
+        counted = jnp.where(mask, fail, 0.0)
+    else:
+        counted = fail
+    sums = jnp.dot(counted.astype(jnp.bfloat16), tri, preferred_element_type=jnp.float32)
+    keys = block_keys.shape[0]
+    both = jnp.concatenate([carry] * (keys // 128), axis=1)
+    weights = jnp.exp2((level - fail) - (sums[:, :keys] + both))
+    if mask is not None:
+        weights = jnp.where(mask, weights, 0.0)
+    out = jnp.dot(weights.astype(jnp.bfloat16), block_values, preferred_element_type=jnp.float32)
+    return out, carry + sums[:, keys:]
+
+
+KEY_TILE = 256
+
+
+def attend_kernel(heads, shard_ref, query_ref, keys_ref, values_ref, bias_ref, tri_ref, out_ref):
+    rows = query_ref.shape[0]
+    size = query_ref.shape[1] // heads
+    pair = 128 // size
+    first_row = shard_ref[0] * rows
+    own_tile = first_row // KEY_TILE
+    tri = tri_ref[...]
+    lane = lax.broadcasted_iota(jnp.int32, (rows, 128), 1)
+    queries = []
+    for head in range(heads):
+        group = query_ref[:, (head // pair) * 128 : (head // pair + 1) * 128] * size**-0.5
+        queries.append(jnp.where(lane // size == head % pair, group, 0).astype(jnp.bfloat16))
+
+    def one_tile(tile, state, masked):
+        start = pl.multiple_of(tile * KEY_TILE, KEY_TILE)
+        if masked:
+            key_pos = start + lax.broadcasted_iota(jnp.int32, (rows, KEY_TILE), 1)
+            query_pos = first_row + lax.broadcasted_iota(jnp.int32, (rows, KEY_TILE), 0)
+            mask = key_pos < query_pos
+        else:
+            mask = None
+        outs, carries = [], []
+        for head in range(heads):
+            columns = slice((head // pair) * 128, (head // pair + 1) * 128)
+            out, carry = stick_block(
+                queries[head],
+                keys_ref[pl.ds(start, KEY_TILE), columns],
+                values_ref[pl.ds(start, KEY_TILE), columns],
+                bias_ref[head : head + 1, pl.ds(start, KEY_TILE)],
+                state[1][head],
+                tri,
+                mask,
+            )
+            outs.append(state[0][head] + out)
+            carries.append(carry)
+        return (tuple(outs), tuple(carries))
+
+    zero = tuple(jnp.zeros((rows, 128), jnp.float32) for _ in range(heads))
+    state = one_tile(own_tile, (zero, zero), True)
+    outs, _ = lax.fori_loop(0, own_tile, lambda turn, state: one_tile(own_tile - 1 - turn, state, False), state)
+    for group in range(heads // pair):
+        merged = outs[group * pair]
+        for other in range(1, pair):
+            merged = jnp.where(lane // size == other, outs[group * pair + other], merged)
+        out_ref[:, group * 128 : (group + 1) * 128] = merged.astype(jnp.bfloat16)
+
+
+def attend(query_rows, all_keys, all_values, all_bias, shard):
+    rows, width = query_rows.shape
+    heads = all_bias.shape[1]
+    row = jnp.arange(KEY_TILE)
+    later = (row[:, None] > row[None, :]).astype(jnp.bfloat16)
+    tri = jnp.concatenate([later, jnp.ones((KEY_TILE, 128), jnp.bfloat16)], axis=1)
+    bias_rows = jnp.transpose(all_bias.astype(jnp.float32))
+    vmem = pl.BlockSpec(memory_space=pltpu.VMEM)
+    return pl.pallas_call(
+        lambda *refs: attend_kernel(heads, *refs),
+        out_shape=jax.ShapeDtypeStruct((rows, width), jnp.bfloat16),
+        in_specs=[pl.BlockSpec(memory_space=pltpu.SMEM)] + [vmem] * 5,
+        out_specs=vmem,
+        compiler_params=pltpu.CompilerParams(vmem_limit_bytes=48 << 20),
+        cost_estimate=pl.CostEstimate(flops=40_000_000_000, bytes_accessed=9_000_000, transcendentals=12_000_000),
+        name="attend",
+    )(jnp.full((1,), shard, jnp.int32), query_rows, all_keys, all_values, bias_rows, tri)
 
 
 def shared_term_of(own_all, shared_gate, shared_up, shared_down):
@@ -89,35 +150,10 @@
     shared_down,
     exit_gain,
 ):
-    shard_rows = query_rows.shape[0]
-    head_count = key_bias.shape[1]
-    head_size = query_rows.shape[1] // head_count
     ep_size = lax.axis_size("ep")
     tp_size = lax.axis_size("tp")
-    own_index = lax.axis_index("ep")
-    query_split = query_rows.reshape(shard_rows, head_count, head_size)
-    query_pos = own_index * shard_rows + jnp.arange(shard_rows, dtype=jnp.int32)
-    span_shards = block_shards(shard_rows, ep_size)
-    empty_output = jnp.zeros((shard_rows, head_count, head_size), jnp.float32)
     all_keys, all_values, all_bias = in_one_piece((key_rows, value_rows, key_bias), "ep", 0, 1)
-    block_rows = span_shards * shard_rows
-    own_block = own_index * shard_rows // block_rows
-
-    def backward_turn(turn_index, carried_pair):
-        output, carried = carried_pair
-        block_start = (own_block - turn_index) * block_rows
-        block_keys = lax.dynamic_slice_in_dim(all_keys, block_start, block_rows, 0)
-        block_values = lax.dynamic_slice_in_dim(all_values, block_start, block_rows, 0)
-        block_bias = lax.dynamic_slice_in_dim(all_bias, block_start, block_rows, 0)
-        scores, fail_logs, causal = break_scores(
-            query_split, block_keys, block_bias, query_pos, block_start
-        )
-        output = output + break_values(scores, fail_logs, causal, carried, block_values)
-        return (output, carried + jnp.sum(fail_logs, axis=2))
-
-    carried_zero = jnp.zeros((head_count, shard_rows), jnp.float32)
-    output, unused = lax.fori_loop(0, own_block + 1, backward_turn, (empty_output, carried_zero))
-    attended = output.reshape(shard_rows, head_count * head_size).astype(jnp.bfloat16)
+    attended = attend(query_rows, all_keys, all_values, all_bias, lax.axis_index("ep"))
     mixer_term = rounded_term(jnp.dot(attended, mixer_weight, preferred_element_type=jnp.float32))
     row_count = routed_input.shape[0]
     top_count = expert_index.shape[1]

time: 451 us -> 344 us (0.76)
  other arithmetic: 121 us -> 14.6 us
  Pallas kernels: 0 us -> 36.4 us
  matrix products: 51.7 us -> 27.2 us
  local copies, waits for them, and re-layouts: 61.6 us -> 54.8 us
    another operation x52 -> x4, other arithmetic: 80.5 us -> 0.2 us
    pallas_call x0 -> x1, Pallas kernels: none -> 36.4 us  [attend(): pl.pallas_call(lambda *refs: attend_kernel(heads, *refs), out_shape=jax.S...]
    convert_element_type x17 -> x0, other arithmetic: 23.8 us -> none  [the longest x16 23.7 us: break_values(): jnp.where(causal, jnp.exp(jax.nn.log_sigmoid(scores) + later_sum), 0.0)]
    dot_general x32 -> x0, matrix products: 23.1 us -> none  [the longest x16 19.5 us: break_scores(): jnp.einsum('qhd,khd->hqk', query_split, keys_split, preferred_element_typ...]
    dynamic_slice x16 -> x0, local copies, waits for them, and re-layouts: 17.1 us -> none  [backward_turn(): block_keys = lax.dynamic_slice_in_dim(all_keys, block_start, block_rows, 0)]
    split x3, local copies, waits for them, and re-layouts: 5.89 us -> 18.6 us  [in_one_piece(): jnp.split(filled, [sum(widths[:k]) for k in range(1, len(widths))], axis=...]
  transfers between devices with their start and end apart: 7 -> 7, of which waited for: 5 -> 5; matrix products, arithmetic and copies ran while one was open for 15% -> 18% of each run, Pallas kernels for 0% -> 0%
where the time goes in v1:
time: 344 us; the launch traced here: 343 us
  waiting for transfers between devices  139 us (40%)
  local copies, waits for them, and re-layouts  54.8 us (16%)
  Pallas kernels  36.4 us (11%)
  blocking collectives  34 us (10%)
  matrix products  27.2 us (8%)
  starting transfers between devices  22.5 us (7%)
  other arithmetic  14.6 us (4%)
  between operations  14.1 us (4%)
    all_to_all x3, waiting for transfers between devices, sum_at_owner(): tiles = lax.all_to_all(in_blocks(array, dim, peers), axis, 0, 0, tiled=True)  66.6 us
    all_gather x1, waiting for transfers between devices, on_device(): lax.all_gather(arrived.reshape(slot_total, model_width), 'tp', axis=0, ti...  48 us
    pallas_call x1, Pallas kernels, attend(): pl.pallas_call(lambda *refs: attend_kernel(heads, *refs), out_shape=jax.S...  36.4 us
    all_to_all x1, blocking collectives, on_device(): lax.all_to_all(outgoing, 'ep', split_axis=0, concat_axis=0, tiled=True)  34 us
    all_to_all x1, waiting for transfers between devices, on_device(): lax.all_to_all(returned_rows, 'ep', split_axis=0, concat_axis=0, tiled=True)  23.5 us
    split x3, local copies, waits for them, and re-layouts, in_one_piece(): jnp.split(filled, [sum(widths[:k]) for k in range(1, len(widths))], axis=...  18.6 us
    convert_element_type x2, local copies, waits for them, and re-layouts, rounded_term(): partial_value.astype(jnp.bfloat16)  16 us
    all_to_all x3, starting transfers between devices, sum_at_owner(): tiles = lax.all_to_all(in_blocks(array, dim, peers), axis, 0, 0, tiled=True)  12.1 us
  transfers between devices with their start and end apart: 7, of which 5 were waited for; matrix products, arithmetic and copies ran while one was open for 18% of the time, Pallas kernels for 0%

profile of v1, /device:TPU:248, one launch (start us, length us, event | category | flops | bytes accessed | tf_op | source)
XLA Modules:
  0.0 342.6 jit_solution(5527814442974879192)
XLA Ops:
  7.2 1.3 fusion.35
  8.6 0.8 copy.56
  9.8 0.2 fusion.49
  10.0 0.1 reduce_sum.80
  10.2 0.7 compare_select_fusion
  10.9 0.7 fusion.45
  11.6 1.2 fusion.37
  12.8 1.2 convolution_convert_fusion.1
  14.1 1.5 reshape.82
  15.6 34.0 %all_to_all.25 = bf16[128,2,2048]{2,1,0:T(2,128)(2,1)S(1)} all-to-all(bf16[128,2,2048]{2,1,0:T(2,128)(2,1)} %reshape.82), channel_id=1, replica_groups=mesh['ep'=64,'tp'=4] {'ep'}, dimensions={0} | all-to-all | bytes 2097152 | tf_op jit(solution)/shard_map/all_to_all | solution.py:176
  49.6 1.2 reshape.83
  50.9 0.7 all-gather.8.cloned.1.call-update
  51.7 1.0 copy.51
  52.6 1.0 copy.52
  53.6 0.7 pad_maximum_fusion
  54.3 48.0 %all-gather.6.cloned.1.call-done = bf16[1024,2048]{1,0:T(8,128)(2,1)} async-done(((bf16[256,2048]{1,0:T(8,128)(2,1)}), bf16[1024,2048]{1,0:T(8,128)(2,1)}) %all-gather.6.cloned.1.call-update) | async-done | bytes 4194320 | tf_op jit(solution)/shard_map/all_gather | solution.py:178
  102.3 7.7 %reshape.84 = bf16[4,64,2,2,2048]{4,3,2,1,0:T(2,128)(2,1)} reshape(bf16[1024,2048]{1,0:T(8,128)(2,1)} %all-gather.6.cloned.1.call-done) | data formatting | bytes 8388608 | tf_op jit(solution)/shard_map/reshape | solution.py:181
  110.0 7.4 %fusion.7 = f32[4,64,2,2,256]{4,1,3,0,2:T(8,128)S(1)} fusion(bf16[2,2048,256]{2,1,0:T(8,128)(2,1)} %param.27, bf16[4,64,2,2,2048]{4,3,2,1,0:T(2,128)(2,1)} %reshape.84), kind=kOutput, calls=%fused_computation.14 | convolution fusion | flops 1073741824 | bytes 7340032 | tf_op jit(solution)/shard_map/tsecd,edf->tsecf/dot_general | solution.py:182
  117.4 10.8 %convert_bitcast_fusion = bf16[4,64,2,2,2048]{4,1,3,0,2:T(8,128)(2,1)} fusion(bf16[2,256,2048]{2,1,0:T(8,128)(2,1)S(1)} %copy-done, bf16[2,2048,256]{2,1,0:T(8,128)(2,1)} %param.28, bf16[4,64,2,2,2048]{4,3,2,1,0:T(2,128)(2,1)} %reshape.84, f32[4,64,2,2,256]{4,1,3,0,2:T(8,128)S(1)} %fusion.7), kind=kOutput, calls=%fused_computation.1 | convolution fusion | flops 2151153664 | bytes 13631488 | tf_op jit(solution)/shard_map/tsecf,efd->tsecd/dot_general | solution.py:189
  128.2 8.8 %copy.62 = bf16[4,64,2,2,2048]{4,3,2,1,0:T(2,128)(2,1)} copy(bf16[4,64,2,2,2048]{4,1,3,0,2:T(8,128)(2,1)} %convert_bitcast_fusion) | data formatting | bytes 8388608 | tf_op jit(solution)/shard_map/convert_element_type | solution.py:34
  137.0 7.2 %convert_element_type.70 = bf16[1024,2048]{1,0:T(8,128)(2,1)} reshape(bf16[4,64,2,2,2048]{4,3,2,1,0:T(2,128)(2,1)} %copy.62) | data formatting | bytes 8388608 | tf_op jit(solution)/shard_map/convert_element_type | solution.py:34
  144.2 5.0 %all-to-all-start.2 = ((bf16[4,256,2048]{2,1,0:T(8,128)(2,1)}), bf16[4,256,2048]{2,1,0:T(8,128)(2,1)}, u32[]{:S(2)}, u32[]{:S(2)}) async-start(bf16[4,256,2048]{2,1,0:T(8,128)(2,1)} %bitcast.61), calls=%async_computation.2 | async-start | bytes 8388608 | tf_op jit(solution)/shard_map/all_to_all | solution.py:25
  149.3 2.1 fusion.53
  151.5 4.5 %convolution_convert_fusion = bf16[384,2048]{1,0:T(8,128)(2,1)} fusion(bf16[256,2048]{1,0:T(8,128)(2,1)} %param.32, bf16[384,2048]{1,0:T(8,128)(2,1)S(1)} %copy-done.11, bf16[2048,256]{1,0:T(8,128)(2,1)} %param.31, f32[384,256]{1,0:T(8,128)S(1)} %fusion.53), kind=kOutput, calls=%fused_computation.7 | convolution fusion | flops 806682624 | bytes 5636096 | tf_op jit(solution)/shard_map/dot_general | solution.py:131
  156.0 42.3 %all-to-all-done.2 = bf16[4,256,2048]{2,1,0:T(8,128)(2,1)} async-done(((bf16[4,256,2048]{2,1,0:T(8,128)(2,1)}), bf16[4,256,2048]{2,1,0:T(8,128)(2,1)}, u32[]{:S(2)}, u32[]{:S(2)}) %all-to-all-start.2) | async-done | bytes 4194336 | tf_op jit(solution)/shard_map/all_to_all | solution.py:25
  198.3 3.6 %all-to-all-start.4 = ((bf16[4,96,2048]{2,1,0:T(8,128)(2,1)}), bf16[4,96,2048]{2,1,0:T(8,128)(2,1)S(1)}, u32[]{:S(2)}, u32[]{:S(2)}) async-start(bf16[4,96,2048]{2,1,0:T(8,128)(2,1)} %bitcast.62), calls=%async_computation.4 | async-start | bytes 3145728 | tf_op jit(solution)/shard_map/all_to_all | solution.py:25
  201.9 3.1 reduce_sum.82
  205.1 1.6 reshape.86
  206.6 15.2 %all-to-all-done.4 = bf16[4,96,2048]{2,1,0:T(8,128)(2,1)S(1)} async-done(((bf16[4,96,2048]{2,1,0:T(8,128)(2,1)}), bf16[4,96,2048]{2,1,0:T(8,128)(2,1)S(1)}, u32[]{:S(2)}, u32[]{:S(2)}) %all-to-all-start.4) | async-done | bytes 1572896 | tf_op jit(solution)/shard_map/all_to_all | solution.py:25
  221.8 10.3 %all-to-all-start.3 = ((bf16[128,2,2048]{2,1,0:T(2,128)(2,1)}), bf16[128,2,2048]{2,1,0:T(2,128)(2,1)S(1)}, u32[]{:S(2)}, u32[]{:S(2)}) async-start(bf16[128,2,2048]{2,1,0:T(2,128)(2,1)} %reshape.86), calls=%async_computation.3 | async-start | bytes 2097152 | tf_op jit(solution)/shard_map/all_to_all | solution.py:200
  232.6 1.1 convert_reduce_fusion
  233.7 23.5 %all-to-all-done.3 = bf16[128,2,2048]{2,1,0:T(2,128)(2,1)S(1)} async-done(((bf16[128,2,2048]{2,1,0:T(2,128)(2,1)}), bf16[128,2,2048]{2,1,0:T(2,128)(2,1)S(1)}, u32[]{:S(2)}, u32[]{:S(2)}) %all-to-all-start.3) | async-done | bytes 1048608 | tf_op jit(solution)/shard_map/all_to_all | solution.py:200
  257.2 0.4 reshape.87
  257.6 1.1 gather_fusion
  258.7 1.0 reshape.100
  259.7 2.3 multiply_reduce_fusion
  262.0 0.2 multiply_reduce_fusion.1
  262.2 5.9 %fusion.52 = (bf16[8192,256]{0,1:T(8,128)(2,1)}, bf16[8192,256]{0,1:T(8,128)(2,1)}) fusion(bf16[8192,516]{0,1:T(8,128)(2,1)} %all-gather.4.cloned.1.call-done), kind=kLoop, calls=%fused_computation.64 | loop fusion | bytes 16777216 | tf_op jit(solution)/shard_map/split | solution.py:15
  268.1 6.4 %copy.54.refs_3_ = bf16[8192,256]{1,0:T(8,128)(2,1)} copy(bf16[8192,256]{0,1:T(8,128)(2,1)} %get-tuple-element.6) | data formatting | bytes 8388608 | tf_op jit(solution)/shard_map/split | solution.py:15
  274.5 6.4 %copy.53.refs_2_ = bf16[8192,256]{1,0:T(8,128)(2,1)} copy(bf16[8192,256]{0,1:T(8,128)(2,1)} %get-tuple-element.7) | data formatting | bytes 8388608 | tf_op jit(solution)/shard_map/split | solution.py:15
  280.9 0.9 convert_bitcast_fusion.1.refs_4_
  281.8 2.2 copy-done.2
  284.0 36.4 %attend.1 = bf16[128,256]{1,0:T(8,128)(2,1)S(1)} custom-call(s32[1]{0:T(128)} %bitcast.refs_0_, bf16[128,256]{1,0:T(8,128)(2,1)S(1)} %copy-done.3, bf16[8192,256]{1,0:T(8,128)(2,1)S(1)} %copy-done.2, bf16[8192,256]{1,0:T(8,128)(2,1)} %copy.54.refs_3_, f32[4,8192]{1,0:T(4,128)S(1)} %convert_bitcast_fusion.1.refs_4_, bf16[256,384]{1,0:T(8,128)(2,1)S(1)} %pad_convert_fusion.refs_5_), custom_call_target="tpu_custom_call" | custom-call | flops 40000000000 | bytes 9000000 | tf_op jit(solution)/shard_map/attend/pallas_call | solution.py:116
  320.5 1.1 convolution_convert_fusion.2
  321.6 3.5 %all-to-all-start = ((bf16[4,32,2048]{2,1,0:T(8,128)(2,1)}), bf16[4,32,2048]{2,1,0:T(8,128)(2,1)S(1)}, u32[]{:S(2)}, u32[]{:S(2)}) async-start(bf16[4,32,2048]{2,1,0:T(8,128)(2,1)} %bitcast.2), calls=%async_computation | async-start | bytes 1048576 | tf_op jit(solution)/shard_map/all_to_all | solution.py:25
  325.1 0.9 multiply_convert_fusion
  326.0 9.1 %all-to-all-done = bf16[4,32,2048]{2,1,0:T(8,128)(2,1)S(1)} async-done(((bf16[4,32,2048]{2,1,0:T(8,128)(2,1)}), bf16[4,32,2048]{2,1,0:T(8,128)(2,1)S(1)}, u32[]{:S(2)}, u32[]{:S(2)}) %all-to-all-start) | async-done | bytes 524320 | tf_op jit(solution)/shard_map/all_to_all | solution.py:25
  335.3 0.8 multiply_convert_fusion.1
  (54 shorter events, 1.4 us)
Async XLA Ops:
  7.2 110.2 %copy-start = (bf16[2,256,2048]{2,1,0:T(8,128)(2,1)S(1)}, bf16[2,256,2048]{2,1,0:T(8,128)(2,1)}, u32[]{:S(2)}) copy-start(bf16[2,256,2048]{2,1,0:T(8,128)(2,1)} %param.29) | copy-start | bytes 6291460
  7.2 95.1 %all-gather.6.cloned.1.call-start = ((), (), s32[]{:S(2)}) async-start(), calls=%async_computation.6 | async-start | bytes 5242880 | tf_op jit(solution)/shard_map/all_gather | solution.py:178
  12.8 36.8 %copy-start.4 = (bf16[96,2048]{1,0:T(8,128)(2,1)}, bf16[96,2048]{1,0:T(8,128)(2,1)S(1)}, u32[]{:S(2)}) copy-start(bf16[96,2048]{1,0:T(8,128)(2,1)S(1)} %fusion.37) | copy-start | bytes 1179652
  49.6 4.0 %copy-start.9 = (bf16[128,4]{0,1:T(4,128)(2,1)S(1)}, bf16[128,4]{0,1:T(4,128)(2,1)}, u32[]{:S(2)}) copy-start(bf16[128,4]{0,1:T(4,128)(2,1)} %param.20) | copy-start | bytes 3076
  50.9 98.4 %all-gather.8.cloned.1.call-start = ((), (), s32[]{:S(2)}) async-start(), calls=%async_computation.7 | async-start | bytes 1966080 | tf_op jit(solution)/shard_map/all_gather | solution.py:179
  51.6 210.6 %all-gather.4.cloned.1.call-start = ((), (), s32[]{:S(2)}) async-start(), calls=%async_computation.5 | async-start | bytes 8652800 | tf_op jit(solution)/shard_map/all_gather | solution.py:14
  144.2 5.1 %copy-start.12 = (bf16[2048,256]{1,0:T(8,128)(2,1)S(1)}, bf16[2048,256]{1,0:T(8,128)(2,1)}, u32[]{:S(2)}) copy-start(bf16[2048,256]{1,0:T(8,128)(2,1)} %param.30) | copy-start | bytes 3145732
  144.2 54.1 %all-to-all-start.2 = ((bf16[4,256,2048]{2,1,0:T(8,128)(2,1)}), bf16[4,256,2048]{2,1,0:T(8,128)(2,1)}, u32[]{:S(2)}, u32[]{:S(2)}) async-start(bf16[4,256,2048]{2,1,0:T(8,128)(2,1)} %bitcast.61), calls=%async_computation.2 | async-start | bytes 8388608 | tf_op jit(solution)/shard_map/all_to_all | solution.py:25
  149.3 2.2 copy-start.11
  198.3 23.6 %all-to-all-start.4 = ((bf16[4,96,2048]{2,1,0:T(8,128)(2,1)}), bf16[4,96,2048]{2,1,0:T(8,128)(2,1)S(1)}, u32[]{:S(2)}, u32[]{:S(2)}) async-start(bf16[4,96,2048]{2,1,0:T(8,128)(2,1)} %bitcast.62), calls=%async_computation.4 | async-start | bytes 3145728 | tf_op jit(solution)/shard_map/all_to_all | solution.py:25
  205.1 27.1 %copy-start.10 = (f32[96,2]{0,1:T(2,128)S(1)}, f32[96,2]{0,1:T(2,128)}, u32[]{:S(2)}) copy-start(f32[96,2]{0,1:T(2,128)} %param.26) | copy-start | bytes 2308
  221.8 35.3 %all-to-all-start.3 = ((bf16[128,2,2048]{2,1,0:T(2,128)(2,1)}), bf16[128,2,2048]{2,1,0:T(2,128)(2,1)S(1)}, u32[]{:S(2)}, u32[]{:S(2)}) async-start(bf16[128,2,2048]{2,1,0:T(2,128)(2,1)} %reshape.86), calls=%async_computation.3 | async-start | bytes 2097152 | tf_op jit(solution)/shard_map/all_to_all | solution.py:200
  259.7 2.3 copy-start.5
  274.5 7.3 %copy-start.3 = (bf16[128,256]{1,0:T(8,128)(2,1)S(1)}, bf16[128,256]{1,0:T(8,128)(2,1)}, u32[]{:S(2)}) copy-start(bf16[128,256]{1,0:T(8,128)(2,1)} %refs_1_.1) | copy-start | bytes 196612
  281.8 2.2 copy-start.2
  284.0 36.4 %copy-start.6 = (bf16[256,2048]{1,0:T(8,128)(2,1)S(1)}, bf16[256,2048]{1,0:T(8,128)(2,1)}, u32[]{:S(2)}) copy-start(bf16[256,2048]{1,0:T(8,128)(2,1)} %param.21) | copy-start | bytes 3145732
  320.5 4.6 %copy-start.7 = (f32[2048]{0:T(1024)S(1)}, f32[2048]{0:T(1024)}, u32[]{:S(2)}) copy-start(f32[2048]{0:T(1024)} %param.33) | copy-start | bytes 24580
  320.5 14.8 %copy-start.8 = (f32[2048]{0:T(1024)S(1)}, f32[2048]{0:T(1024)}, u32[]{:S(2)}) copy-start(f32[2048]{0:T(1024)} %param.22) | copy-start | bytes 24580
  320.5 15.6 %copy-start.1 = (bf16[2,256,2048]{2,1,0:T(8,128)(2,1)S(1)}, bf16[2,256,2048]{2,1,0:T(8,128)(2,1)}, u32[]{:S(2)}) copy-start(bf16[2,256,2048]{2,1,0:T(8,128)(2,1)} %param.29) | copy-start | bytes 6291460
  321.6 13.5 %all-to-all-start = ((bf16[4,32,2048]{2,1,0:T(8,128)(2,1)}), bf16[4,32,2048]{2,1,0:T(8,128)(2,1)S(1)}, u32[]{:S(2)}, u32[]{:S(2)}) async-start(bf16[4,32,2048]{2,1,0:T(8,128)(2,1)} %bitcast.2), calls=%async_computation | async-start | bytes 1048576 | tf_op jit(solution)/shard_map/all_to_all | solution.py:25
Sparse Core Ops, SparseCore 0:
  51.0 51.2 all-gather.5
  104.7 29.3 all-gather.7
  136.7 85.6 all-gather.3

commit v2 on v1

--- a/solution.py
+++ b/solution.py
@@ -1,3 +1,5 @@
+import functools
+
 import jax
 import jax.numpy as jnp
 from jax import lax
@@ -124,11 +126,472 @@
     )(jnp.full((1,), shard, jnp.int32), query_rows, all_keys, all_values, bias_rows, tri)
 
 
-def shared_term_of(own_all, shared_gate, shared_up, shared_down):
-    gate_part = jnp.dot(own_all, shared_gate, preferred_element_type=jnp.float32)
-    up_part = jnp.dot(own_all, shared_up, preferred_element_type=jnp.float32)
-    hidden = (jax.nn.silu(gate_part) * up_part).astype(jnp.bfloat16)
-    return rounded_term(jnp.dot(hidden, shared_down, preferred_element_type=jnp.float32))
+PLANE = 8
+CAPACITY = 2
+
+
+def silu_product(gate, up):
+    return (gate / (1.0 + jnp.exp(-gate)) * up).astype(jnp.bfloat16)
+
+
+def expert_kernel(
+    groups,
+    plane,
+    outgoing,
+    normed,
+    gate_hbm,
+    up_hbm,
+    down_hbm,
+    shared_gate_hbm,
+    shared_up_hbm,
+    shared_down_hbm,
+    back,
+    shared_out,
+    stage,
+    rows,
+    partial,
+    first_sum,
+    second_sum,
+    result,
+    returned,
+    neighbours,
+    shared_part,
+    shared_first,
+    shared_second,
+    gate_w,
+    up_w,
+    down_w,
+    shared_gate_w,
+    shared_up_w,
+    shared_down_w,
+    weight_sem,
+    own_sem,
+    z_send,
+    z_recv,
+    p_send,
+    p_recv,
+    x_send,
+    x_recv,
+    q_send,
+    q_recv,
+    b_send,
+    b_recv,
+    s_send,
+    s_recv,
+):
+    f32, bf16 = jnp.float32, jnp.bfloat16
+    own_ep = lax.axis_index("ep")
+    own_x = lax.axis_index("tp")
+    own_z = own_ep // plane
+    own_p = own_ep % plane
+    half = plane // 2
+    right = (own_x + 1) % 4
+    left = (own_x + 3) % 4
+    side = (right, left)
+    experts, width = gate_w.shape[0], gate_w.shape[1]
+    shared_rows = normed.shape[0]
+    shared_half = shared_rows // 2
+
+    def remote(src, dst, send_sem, recv_sem, ep, tp):
+        return pltpu.make_async_remote_copy(
+            src_ref=src,
+            dst_ref=dst,
+            send_sem=send_sem,
+            recv_sem=recv_sem,
+            device_id=(ep, tp),
+            device_id_type=pl.DeviceIdType.MESH,
+        )
+
+    def offset(c):
+        odd = c % 2
+        return (odd * ((c + 1) // 2) + (1 - odd) * (groups - c // 2)) % groups
+
+    def z_copy(c):
+        there = (own_z + offset(c)) % groups
+        return remote(
+            outgoing.at[there], stage.at[c], z_send.at[c], z_recv.at[c], there * plane + own_p, own_x
+        )
+
+    def p_copy(c, i):
+        there = (own_p + i) % plane
+        return remote(
+            stage.at[c, there],
+            rows.at[0, c, own_p],
+            p_send.at[c, i],
+            p_recv.at[c, i],
+            own_z * plane + there,
+            own_x,
+        )
+
+    def p_own(c):
+        return pltpu.make_async_copy(stage.at[c, own_p], rows.at[0, c, own_p], own_sem.at[0, c])
+
+    def x_copy(c, way):
+        return remote(
+            rows.at[0, c], rows.at[1 + way, c], x_send.at[0, way, c], x_recv.at[0, way, c], own_ep, side[way]
+        )
+
+    def f_copy(c, way):
+        part = pl.ds(way * half, half)
+        return remote(
+            rows.at[1 + way, c, part],
+            rows.at[3, c, part],
+            x_send.at[1, way, c],
+            x_recv.at[1, way, c],
+            own_ep,
+            side[way],
+        )
+
+    def r_copy(c, way):
+        return remote(
+            partial.at[3, c, pl.ds(way * half, half)],
+            first_sum.at[way, c],
+            x_send.at[2, way, c],
+            x_recv.at[2, way, c],
+            own_ep,
+            side[way],
+        )
+
+    def t_copy(c, way):
+        return remote(
+            partial.at[2 - way, c],
+            second_sum.at[way, c],
+            x_send.at[3, way, c],
+            x_recv.at[3, way, c],
+            own_ep,
+            side[way],
+        )
+
+    def q_copy(c, i):
+        there = (own_p + i) % plane
+        return remote(
+            result.at[c, there],
+            returned.at[c, own_p],
+            q_send.at[c, i],
+            q_recv.at[c, i],
+            own_z * plane + there,
+            own_x,
+        )
+
+    def q_own(c):
+        return pltpu.make_async_copy(result.at[c, own_p], returned.at[c, own_p], own_sem.at[1, c])
+
+    def b_copy(c):
+        there = (own_z + groups - offset(c)) % groups
+        return remote(
+            returned.at[c], back.at[own_z], b_send.at[c], b_recv.at[c], there * plane + own_p, own_x
+        )
+
+    def shared_copy(kind, way):
+        part = pl.ds(way * shared_half, shared_half)
+        src, dst = (
+            (normed, neighbours.at[way]),
+            (neighbours.at[way, part], neighbours.at[2, part]),
+            (shared_part.at[3, part], shared_first.at[way]),
+            (shared_part.at[2 - way], shared_second.at[way]),
+        )[kind]
+        return remote(src, dst, s_send.at[kind, way], s_recv.at[kind, way], own_ep, side[way])
+
+    first_z = pltpu.make_async_copy(outgoing.at[own_z], stage.at[0], own_sem.at[2, 0])
+    last_z = pltpu.make_async_copy(returned.at[0], back.at[own_z], own_sem.at[2, 1])
+    loads = [
+        pltpu.make_async_copy(src, dst, weight_sem.at[n])
+        for n, (src, dst) in enumerate(
+            (
+                (shared_gate_hbm, shared_gate_w),
+                (shared_up_hbm, shared_up_w),
+                (shared_down_hbm, shared_down_w),
+                (gate_hbm, gate_w),
+                (up_hbm, up_w),
+                (down_hbm, down_w),
+            )
+        )
+    ]
+
+    barrier = pltpu.get_barrier_semaphore()
+
+    def greet(ep, tp):
+        pl.semaphore_signal(
+            barrier, inc=1, device_id=(ep, tp), device_id_type=pl.DeviceIdType.MESH
+        )
+
+    for k in range(1, groups):
+        greet(((own_z + k) % groups) * plane + own_p, own_x)
+    for k in range(1, plane):
+        greet(own_z * plane + (own_p + k) % plane, own_x)
+    greet(own_ep, right)
+    greet(own_ep, left)
+    first_z.start()
+    for load in loads:
+        load.start()
+    pl.semaphore_wait(barrier, groups + plane)
+
+    for way in range(2):
+        shared_copy(0, way).start()
+    for c in range(1, groups):
+        z_copy(c).start()
+    first_z.wait()
+
+    def compute_shared():
+        def one_block(source, target):
+            block = source[...]
+            gate = jnp.dot(block, shared_gate_w[...], preferred_element_type=f32)
+            up = jnp.dot(block, shared_up_w[...], preferred_element_type=f32)
+            hidden = silu_product(gate, up)
+            target[...] = jnp.dot(hidden, shared_down_w[...], preferred_element_type=f32).astype(bf16)
+
+        one_block(normed, shared_part.at[0])
+        for j in range(3):
+            one_block(neighbours.at[j], shared_part.at[j + 1])
+
+    def compute_rows(c):
+        count = 4 * plane * CAPACITY
+        for e in range(experts):
+            block = rows[:, c, :, e].reshape(count, width)
+            gate = jnp.dot(block, gate_w[e], preferred_element_type=f32)
+            up = jnp.dot(block, up_w[e], preferred_element_type=f32)
+            hidden = silu_product(gate, up)
+            product = jnp.dot(hidden, down_w[e], preferred_element_type=f32).astype(bf16)
+            partial[:, c, :, e] = product.reshape(4, plane, CAPACITY, width)
+
+    def flat(value):
+        return value.reshape(-1, width).astype(f32)
+
+    def add_first(c):
+        for way in range(2):
+            part = pl.ds(way * half, half)
+            total = flat(partial[2 - way, c, part]) + flat(first_sum[way, c])
+            partial[2 - way, c, part] = total.astype(bf16).reshape(half, experts, CAPACITY, width)
+
+    def add_second(c):
+        total = flat(partial[0, c]) + flat(second_sum[0, c]) + flat(second_sum[1, c])
+        result[c] = total.astype(bf16).reshape(plane, experts, CAPACITY, width)
+
+    def step(s, unused):
+        @pl.when(s < groups)
+        def _():
+            @pl.when(s > 0)
+            def _():
+                z_copy(s).wait_recv()
+
+            p_own(s).start()
+            for i in range(1, plane):
+                p_copy(s, i).start()
+
+        @pl.when(s == 2)
+        def _():
+            for way in range(2):
+                shared_copy(0, way).wait_recv()
+                shared_copy(1, way).start()
+
+        @pl.when((s >= 1) & (s < groups + 1))
+        def _():
+            c = s - 1
+            for i in range(1, plane):
+                p_copy(c, i).wait_recv()
+            p_own(c).wait()
+            for way in range(2):
+                x_copy(c, way).start()
+
+        @pl.when((s >= 2) & (s < groups + 2))
+        def _():
+            c = s - 2
+            for way in range(2):
+                x_copy(c, way).wait_recv()
+                f_copy(c, way).start()
+
+        @pl.when(s == 3)
+        def _():
+            for load in loads:
+                load.wait()
+            for way in range(2):
+                shared_copy(1, way).wait_recv()
+            compute_shared()
+
+        @pl.when((s >= 3) & (s < groups + 3))
+        def _():
+            c = s - 3
+            for way in range(2):
+                f_copy(c, way).wait_recv()
+            compute_rows(c)
+            for way in range(2):
+                r_copy(c, way).start()
+
+        @pl.when(s == groups)
+        def _():
+            for way in range(2):
+                shared_copy(2, way).start()
+
+        @pl.when((s >= 4) & (s < groups + 4))
+        def _():
+            c = s - 4
+            for way in range(2):
+                r_copy(c, way).wait_recv()
+            add_first(c)
+            for way in range(2):
+                t_copy(c, way).start()
+
+        @pl.when(s == groups + 1)
+        def _():
+            for way in range(2):
+                shared_copy(2, way).wait_recv()
+                part = pl.ds(way * shared_half, shared_half)
+                shared_part[2 - way, part] = (
+                    shared_part[2 - way, part].astype(f32) + shared_first[way].astype(f32)
+                ).astype(bf16)
+            for way in range(2):
+                shared_copy(3, way).start()
+
+        @pl.when((s >= 5) & (s < groups + 5))
+        def _():
+            c = s - 5
+            for way in range(2):
+                t_copy(c, way).wait_recv()
+            add_second(c)
+            q_own(c).start()
+            for i in range(1, plane):
+                q_copy(c, i).start()
+
+        @pl.when((s >= 6) & (s < groups + 6))
+        def _():
+            c = s - 6
+            for i in range(1, plane):
+                q_copy(c, i).wait_recv()
+            q_own(c).wait()
+
+            @pl.when(c > 0)
+            def _():
+                b_copy(c).start()
+
+            @pl.when(c == 0)
+            def _():
+                last_z.start()
+
+        return unused
+
+    lax.fori_loop(0, groups + 6, step, 0)
+
+    for way in range(2):
+        shared_copy(3, way).wait_recv()
+    shared_out[...] = (
+        shared_part[0].astype(f32) + shared_second[0].astype(f32) + shared_second[1].astype(f32)
+    )
+
+    def drain(c, unused):
+        for i in range(1, plane):
+            p_copy(c, i).wait_send()
+            q_copy(c, i).wait_send()
+        for way in range(2):
+            for copy in (x_copy, f_copy, r_copy, t_copy):
+                copy(c, way).wait_send()
+
+        @pl.when(c > 0)
+        def _():
+            z_copy(c).wait_send()
+            b_copy(c).wait_send()
+            b_copy(c).wait_recv()
+
+        return unused
+
+    lax.fori_loop(0, groups, drain, 0)
+    for kind in range(4):
+        for way in range(2):
+            shared_copy(kind, way).wait_send()
+    last_z.wait()
+
+
+def exchange_and_expand(outgoing, normed, gate, up, down, shared_gate, shared_up, shared_down):
+    groups, plane, experts, capacity, width = outgoing.shape
+    count = normed.shape[0]
+    half = plane // 2
+    bf16 = jnp.bfloat16
+    block = (plane, experts, capacity, width)
+    vmem = pl.BlockSpec(memory_space=pltpu.VMEM)
+    hbm = pl.BlockSpec(memory_space=pl.ANY)
+    weights = (gate, up, down, shared_gate, shared_up, shared_down)
+    dma = pltpu.SemaphoreType.DMA
+    return pl.pallas_call(
+        functools.partial(expert_kernel, groups, plane),
+        out_shape=(
+            jax.ShapeDtypeStruct(outgoing.shape, bf16),
+            jax.ShapeDtypeStruct(normed.shape, jnp.float32),
+        ),
+        in_specs=[vmem, vmem] + [hbm] * 6,
+        out_specs=(vmem, vmem),
+        scratch_shapes=[
+            pltpu.VMEM((groups,) + block, bf16),
+            pltpu.VMEM((4, groups) + block, bf16),
+            pltpu.VMEM((4, groups) + block, bf16),
+            pltpu.VMEM((2, groups, half) + block[1:], bf16),
+            pltpu.VMEM((2, groups) + block, bf16),
+            pltpu.VMEM((groups,) + block, bf16),
+            pltpu.VMEM((groups,) + block, bf16),
+            pltpu.VMEM((3, count, width), bf16),
+            pltpu.VMEM((4, count, width), bf16),
+            pltpu.VMEM((2, count // 2, width), bf16),
+            pltpu.VMEM((2, count, width), bf16),
+        ]
+        + [pltpu.VMEM(w.shape, bf16) for w in weights]
+        + [
+            dma((6,)),
+            dma((3, groups)),
+            dma((groups,)),
+            dma((groups,)),
+            dma((groups, plane)),
+            dma((groups, plane)),
+            dma((4, 2, groups)),
+            dma((4, 2, groups)),
+            dma((groups, plane)),
+            dma((groups, plane)),
+            dma((groups,)),
+            dma((groups,)),
+            dma((4, 2)),
+            dma((4, 2)),
+        ],
+        compiler_params=pltpu.CompilerParams(
+            collective_id=1, has_side_effects=True, vmem_limit_bytes=60 << 20
+        ),
+        name="experts",
+    )(outgoing, normed, *weights)
+
+
+def expert_layer(
+    routed_input,
+    entry_gain,
+    expert_index,
+    route_weights,
+    expert_gate,
+    expert_up,
+    expert_down,
+    shared_gate,
+    shared_up,
+    shared_down,
+    exit_gain,
+):
+    ep_size = lax.axis_size("ep")
+    row_count, top_count = expert_index.shape
+    local_experts = expert_gate.shape[0]
+    model_width = routed_input.shape[1]
+    expert_count = local_experts * ep_size
+    slot_total = expert_count * CAPACITY
+    normed = root_norm(routed_input.astype(jnp.float32), entry_gain).astype(jnp.bfloat16)
+    flat_expert = expert_index.reshape(-1)
+    onehot = (flat_expert[:, None] == jnp.arange(expert_count, dtype=jnp.int32)[None, :]).astype(
+        jnp.int32
+    )
+    slot_rank = jnp.sum((jnp.cumsum(onehot, axis=0) - onehot) * onehot, axis=1)
+    slot_index = (flat_expert * CAPACITY + slot_rank).reshape(row_count, top_count)
+    matches = slot_index[None, :, :] == jnp.arange(slot_total, dtype=jnp.int32)[:, None, None]
+    selector = jnp.any(matches, axis=2).astype(jnp.bfloat16)
+    outgoing = jnp.dot(selector, normed, preferred_element_type=jnp.float32).astype(jnp.bfloat16)
+    outgoing = outgoing.reshape(ep_size // PLANE, PLANE, local_experts, CAPACITY, model_width)
+    back, shared_sum = exchange_and_expand(
+        outgoing, normed, expert_gate, expert_up, expert_down, shared_gate, shared_up, shared_down
+    )
+    back_rows = back.reshape(slot_total, model_width)
+    gathered = back_rows[slot_index].astype(jnp.float32)
+    routed = jnp.sum(route_weights[:, :, None] * gathered, axis=1)
+    return root_norm(routed + shared_sum, exit_gain).astype(jnp.bfloat16)
 
 
 def on_device(
@@ -150,60 +613,23 @@
     shared_down,
     exit_gain,
 ):
-    ep_size = lax.axis_size("ep")
-    tp_size = lax.axis_size("tp")
     all_keys, all_values, all_bias = in_one_piece((key_rows, value_rows, key_bias), "ep", 0, 1)
     attended = attend(query_rows, all_keys, all_values, all_bias, lax.axis_index("ep"))
     mixer_term = rounded_term(jnp.dot(attended, mixer_weight, preferred_element_type=jnp.float32))
-    row_count = routed_input.shape[0]
-    top_count = expert_index.shape[1]
-    local_experts = expert_gate.shape[0]
-    model_width = routed_input.shape[1]
-    expert_count = local_experts * ep_size
-    capacity = 3 * row_count * top_count // (2 * expert_count)
-    slot_total = expert_count * capacity
-    normed = root_norm(routed_input.astype(jnp.float32), entry_gain).astype(jnp.bfloat16)
-    flat_expert = expert_index.reshape(-1)
-    onehot = (flat_expert[:, None] == jnp.arange(expert_count, dtype=jnp.int32)[None, :]).astype(
-        jnp.int32
+    mixer_sum = sum_at_owner(mixer_term.astype(jnp.bfloat16), "tp", 0)
+    expert_out = expert_layer(
+        routed_input,
+        entry_gain,
+        expert_index,
+        route_weights,
+        expert_gate,
+        expert_up,
+        expert_down,
+        shared_gate,
+        shared_up,
+        shared_down,
+        exit_gain,
     )
-    slot_rank = jnp.sum((jnp.cumsum(onehot, axis=0) - onehot) * onehot, axis=1)
-    slot_index = (flat_expert * capacity + slot_rank).reshape(row_count, top_count)
-    matches = slot_index[None, :, :] == jnp.arange(slot_total, dtype=jnp.int32)[:, None, None]
-    selector = jnp.any(matches, axis=2).astype(jnp.bfloat16)
-    outgoing = jnp.dot(selector, normed, preferred_element_type=jnp.float32).astype(jnp.bfloat16)
-    outgoing = outgoing.reshape(expert_count, capacity, model_width)
-    arrived = lax.all_to_all(outgoing, "ep", split_axis=0, concat_axis=0, tiled=True)
-    routed_all, own_all = (
-        lax.all_gather(arrived.reshape(slot_total, model_width), "tp", axis=0, tiled=True),
-        lax.all_gather(normed, "tp", axis=0, tiled=True),
-    )
-    routed_split = routed_all.reshape(tp_size, ep_size, local_experts, capacity, model_width)
-    gate_part = jnp.einsum(
-        "tsecd,edf->tsecf", routed_split, expert_gate, preferred_element_type=jnp.float32
-    )
-    up_part = jnp.einsum(
-        "tsecd,edf->tsecf", routed_split, expert_up, preferred_element_type=jnp.float32
-    )
-    hidden = (jax.nn.silu(gate_part) * up_part).astype(jnp.bfloat16)
-    routed_term = jnp.einsum(
-        "tsecf,efd->tsecd", hidden, expert_down, preferred_element_type=jnp.float32
-    )
-    routed_term = rounded_term(routed_term.reshape(tp_size * slot_total, model_width))
-    shared_term = shared_term_of(own_all, shared_gate, shared_up, shared_down)
-    mixer_sum, routed_sum, shared_sum = (
-        sum_at_owner(mixer_term.astype(jnp.bfloat16), "tp", 0),
-        sum_at_owner(routed_term.astype(jnp.bfloat16), "tp", 0),
-        sum_at_owner(shared_term.astype(jnp.bfloat16), "tp", 0),
-    )
-    returned_rows = routed_sum.astype(jnp.bfloat16).reshape(expert_count, capacity, model_width)
-    back_rows = lax.all_to_all(
-        returned_rows, "ep", split_axis=0, concat_axis=0, tiled=True
-    ).reshape(slot_total, model_width)
-    gathered = back_rows[slot_index].astype(jnp.float32)
-    routed = jnp.sum(route_weights[:, :, None] * gathered, axis=1)
-    combined = routed + shared_sum
-    expert_out = root_norm(combined, exit_gain).astype(jnp.bfloat16)
     mixer_out = root_norm(mixer_sum, mixer_gain).astype(jnp.bfloat16)
     return (mixer_out, expert_out)
 

time: 344 us -> 230 us (0.67)
  waiting for transfers between devices: 139 us -> 8.31 us
  Pallas kernels: 36.4 us -> 156 us
  blocking collectives: 34 us -> 0 us
  matrix products: 27.2 us -> 1.58 us
  local copies, waits for them, and re-layouts: 54.8 us -> 32.2 us
  starting transfers between devices: 22.5 us -> 3.51 us
    pallas_call x0 -> x1, Pallas kernels: none -> 119 us  [exchange_and_expand(): pl.pallas_call(functools.partial(expert_kernel, groups, plane), out_shape...]
    all_to_all x3 -> x1, waiting for transfers between devices: 66.6 us -> 8.27 us  [sum_at_owner(): tiles = lax.all_to_all(in_blocks(array, dim, peers), axis, 0, 0, tiled=True)]
    all_gather x2 -> x0, waiting for transfers between devices: 48 us -> none  [the longest x1 48 us: on_device(): lax.all_gather(arrived.reshape(slot_total, model_width), 'tp', axis=0, ti...]
    all_to_all x1 -> x0, blocking collectives: 34 us -> none  [on_device(): lax.all_to_all(outgoing, 'ep', split_axis=0, concat_axis=0, tiled=True)]
    dot_general x5 -> x1, matrix products: 26.1 us -> 0.48 us  [expert_layer(): jnp.dot(selector, normed, preferred_element_type=jnp.float32)]
    all_to_all x1 -> x0, waiting for transfers between devices: 23.5 us -> none  [on_device(): lax.all_to_all(returned_rows, 'ep', split_axis=0, concat_axis=0, tiled=True)]
    convert_element_type x3 -> x1, local copies, waits for them, and re-layouts: 16.9 us -> 2.15 us  [expert_layer(): gathered = back_rows[slot_index].astype(jnp.float32)]
    all_to_all x1 -> x0, starting transfers between devices: 10.3 us -> none  [on_device(): lax.all_to_all(returned_rows, 'ep', split_axis=0, concat_axis=0, tiled=True)]
  transfers between devices with their start and end apart: 7 -> 2, of which waited for: 5 -> 1; matrix products, arithmetic and copies ran while one was open for 18% -> 8% of each run, Pallas kernels for 0% -> 53%
where the time goes in v2:
time: 230 us; the launch traced here: 227 us
  Pallas kernels  156 us (68%)
  local copies, waits for them, and re-layouts  32.2 us (14%)
  between operations  14.3 us (6%)
  other arithmetic  11.4 us (5%)
  waiting for transfers between devices  8.31 us (4%)
  starting transfers between devices  3.51 us (2%)
    pallas_call x1, Pallas kernels, exchange_and_expand(): pl.pallas_call(functools.partial(expert_kernel, groups, plane), out_shape...  119 us
    pallas_call x1, Pallas kernels, attend(): pl.pallas_call(lambda *refs: attend_kernel(heads, *refs), out_shape=jax.S...  36.4 us
    split x3, local copies, waits for them, and re-layouts, in_one_piece(): jnp.split(filled, [sum(widths[:k]) for k in range(1, len(widths))], axis=...  18.6 us
    all_to_all x1, waiting for transfers between devices, sum_at_owner(): tiles = lax.all_to_all(in_blocks(array, dim, peers), axis, 0, 0, tiled=True)  8.27 us
    unnamed x17, local copies, waits for them, and re-layouts  5.75 us
  transfers between devices with their start and end apart: 2, of which 1 were waited for; matrix products, arithmetic and copies ran while one was open for 8% of the time, Pallas kernels for 53%

profile of v2, /device:TPU:248, one launch (start us, length us, event | category | flops | bytes accessed | tf_op | source)
XLA Modules:
  0.0 227.1 jit_solution(16345805657618746095)
XLA Ops:
  7.2 0.0 copy-start
  7.2 0.0 all-gather.2.cloned.1.call-start
  7.2 1.0 copy.46
  8.3 1.0 copy.47
  9.2 1.3 pad_maximum_fusion
  10.6 0.0 all-gather.2.cloned.1.call-update
  10.6 0.8 copy.50
  11.4 0.8 copy.51
  12.1 0.1 eq.35
  12.3 0.1 iota_compare_fusion.2
  12.4 0.1 fusion.4
  12.6 0.2 fusion.7
  12.8 0.1 reduce_sum.59
  13.0 0.1 copy.54
  13.0 0.7 compare_select_fusion
  13.7 0.1 copy.55
  13.8 0.1 reshape.70
  14.0 0.1 fusion.3
  14.1 1.2 fusion
  15.3 1.2 fusion.2.normed
  16.4 0.0 copy-start.3
  16.5 0.5 convolution_convert_fusion
  16.9 1.5 reshape.65.outgoing
  18.5 0.0 copy-done.3
  18.5 119.4 %experts.1 = (bf16[8,8,2,2,2048]{4,3,2,1,0:T(2,128)(2,1)}, f32[96,2048]{1,0:T(8,128)}) custom-call(bf16[8,8,2,2,2048]{4,3,2,1,0:T(2,128)(2,1)} %reshape.65.outgoing, bf16[96,2048]{1,0:T(8,128)(2,1)} %copy-done.3, bf16[2,2048,256]{2,1,0:T(8,128)(2,1)} %gate_hbm.1, bf16[2,2048,256]{2,1,0:T(8,128)(2,1)} %up_hbm.1, bf16[2,256,2048]{2,1,0:T(8,128)(2,1)} %down_hbm.1, ...), custom_call_target="tpu_custom_call" | custom-call | tf_op jit(solution)/shard_map/experts/pallas_call | solution.py:513
  137.9 1.5 reshape.66
  139.4 2.1 gather_fusion
  141.4 2.1 reshape.78
  143.7 2.3 %multiply_reduce_fusion = f32[96,2048]{1,0:T(8,128)S(1)} fusion(f32[96,2,2048]{2,1,0:T(2,128)S(1)} %reshape.78, f32[96,2]{1,0:T(8,128)S(1)} %copy.50), kind=kLoop, calls=%fused_computation.3 | loop fusion | flops 589824 | bytes 2360064 | tf_op jit(solution)/shard_map/reduce_sum | solution.py:593
  146.0 1.3 multiply_reduce_fusion.1
  147.3 0.0 all-gather.2.cloned.1.call-done
  147.3 5.9 %fusion.8 = (bf16[8192,256]{0,1:T(8,128)(2,1)}, bf16[8192,256]{0,1:T(8,128)(2,1)}) fusion(bf16[8192,516]{0,1:T(8,128)(2,1)} %all-gather.2.cloned.1.call-done), kind=kLoop, calls=%fused_computation.36 | loop fusion | bytes 16777216 | tf_op jit(solution)/shard_map/split | solution.py:17
  153.2 6.4 %copy.49.refs_3_ = bf16[8192,256]{1,0:T(8,128)(2,1)} copy(bf16[8192,256]{0,1:T(8,128)(2,1)} %get-tuple-element.10) | data formatting | bytes 8388608 | tf_op jit(solution)/shard_map/split | solution.py:17
  159.6 6.4 %copy.48.refs_2_ = bf16[8192,256]{1,0:T(8,128)(2,1)} copy(bf16[8192,256]{0,1:T(8,128)(2,1)} %get-tuple-element.11) | data formatting | bytes 8388608 | tf_op jit(solution)/shard_map/split | solution.py:17
  166.0 0.9 convert_bitcast_fusion.refs_4_
  166.9 0.0 copy-done.2
  166.9 0.0 copy-start.1
  166.9 2.2 copy-done.1
  169.1 36.4 %attend.1 = bf16[128,256]{1,0:T(8,128)(2,1)S(1)} custom-call(s32[1]{0:T(128)} %bitcast.refs_0_, bf16[128,256]{1,0:T(8,128)(2,1)S(1)} %copy-done.2, bf16[8192,256]{1,0:T(8,128)(2,1)S(1)} %copy-done.1, bf16[8192,256]{1,0:T(8,128)(2,1)} %copy.49.refs_3_, f32[4,8192]{1,0:T(4,128)S(1)} %convert_bitcast_fusion.refs_4_, bf16[256,384]{1,0:T(8,128)(2,1)S(1)} %pad_convert_fusion.refs_5_), custom_call_target="tpu_custom_call" | custom-call | flops 40000000000 | bytes 9000000 | tf_op jit(solution)/shard_map/attend/pallas_call | solution.py:118
  205.5 0.0 copy-done
  205.5 0.0 copy-start.5
  205.5 1.1 convolution_convert_fusion.1
  206.6 3.5 %all-to-all-start = ((bf16[4,32,2048]{2,1,0:T(8,128)(2,1)}), bf16[4,32,2048]{2,1,0:T(8,128)(2,1)S(1)}, u32[]{:S(2)}, u32[]{:S(2)}) async-start(bf16[4,32,2048]{2,1,0:T(8,128)(2,1)} %bitcast.2), calls=%async_computation | async-start | bytes 1048576 | tf_op jit(solution)/shard_map/all_to_all | solution.py:27
  210.1 0.9 multiply_convert_fusion
  211.0 8.3 %all-to-all-done = bf16[4,32,2048]{2,1,0:T(8,128)(2,1)S(1)} async-done(((bf16[4,32,2048]{2,1,0:T(8,128)(2,1)}), bf16[4,32,2048]{2,1,0:T(8,128)(2,1)S(1)}, u32[]{:S(2)}, u32[]{:S(2)}) %all-to-all-start) | async-done | bytes 524320 | tf_op jit(solution)/shard_map/all_to_all | solution.py:27
  219.2 0.1 convert_reduce_fusion
  219.3 0.1 multiply_reduce_fusion.2
  219.5 0.8 multiply_convert_fusion.1
  (17 shorter events, 0.2 us)
Async XLA Ops:
  7.2 198.3 %copy-start = (bf16[256,2048]{1,0:T(8,128)(2,1)S(1)}, bf16[256,2048]{1,0:T(8,128)(2,1)}, u32[]{:S(2)}) copy-start(bf16[256,2048]{1,0:T(8,128)(2,1)} %param.21) | copy-start | bytes 3145732
  7.2 140.2 %all-gather.2.cloned.1.call-start = ((), (), s32[]{:S(2)}) async-start(), calls=%async_computation.1 | async-start | bytes 8652800 | tf_op jit(solution)/shard_map/all_gather | solution.py:16
  16.4 2.0 copy-start.3
  159.6 7.3 %copy-start.2 = (bf16[128,256]{1,0:T(8,128)(2,1)S(1)}, bf16[128,256]{1,0:T(8,128)(2,1)}, u32[]{:S(2)}) copy-start(bf16[128,256]{1,0:T(8,128)(2,1)} %refs_1_.1) | copy-start | bytes 196612
  166.9 2.2 copy-start.1
  169.1 41.0 %copy-start.4 = (f32[2048]{0:T(1024)S(1)}, f32[2048]{0:T(1024)}, u32[]{:S(2)}) copy-start(f32[2048]{0:T(1024)} %param.33) | copy-start | bytes 24580
  205.5 14.0 %copy-start.5 = (f32[2048]{0:T(1024)S(1)}, f32[2048]{0:T(1024)}, u32[]{:S(2)}) copy-start(f32[2048]{0:T(1024)} %param.22) | copy-start | bytes 24580
  206.6 12.6 %all-to-all-start = ((bf16[4,32,2048]{2,1,0:T(8,128)(2,1)}), bf16[4,32,2048]{2,1,0:T(8,128)(2,1)S(1)}, u32[]{:S(2)}, u32[]{:S(2)}) async-start(bf16[4,32,2048]{2,1,0:T(8,128)(2,1)} %bitcast.2), calls=%async_computation | async-start | bytes 1048576 | tf_op jit(solution)/shard_map/all_to_all | solution.py:27
Sparse Core Ops, SparseCore 0:
  10.7 102.8 all-gather.1

commit v3 on v2

v3 whole, which is shorter than its diff:
```python
import functools

import jax
import jax.numpy as jnp
from jax import lax
from jax.experimental import pallas as pl
from jax.experimental.pallas import tpu as pltpu
from jax.sharding import PartitionSpec as P

EPS = 1e-06
LOG2E = 1.4426950408889634
PLANE = 8
CAPACITY = 2


def root_norm(values, gain_row):
    return values * lax.rsqrt(jnp.mean(values * values, axis=-1, keepdims=True) + EPS) * gain_row


def stick_block(query, block_keys, block_values, bias, carry, tri, mask):
    scores = lax.dot_general(query, block_keys, (((1,), (1,)), ((), ())), preferred_element_type=jnp.float32)
    level = (scores + bias) * LOG2E
    fail = jnp.maximum(level, 0.0) + jnp.log2(1.0 + jnp.exp2(-jnp.abs(level)))
    if mask is not None:
        counted = jnp.where(mask, fail, 0.0)
    else:
        counted = fail
    sums = jnp.dot(counted.astype(jnp.bfloat16), tri, preferred_element_type=jnp.float32)
    keys = block_keys.shape[0]
    both = jnp.concatenate([carry] * (keys // 128), axis=1)
    weights = jnp.exp2((level - fail) - (sums[:, :keys] + both))
    if mask is not None:
        weights = jnp.where(mask, weights, 0.0)
    out = jnp.dot(weights.astype(jnp.bfloat16), block_values, preferred_element_type=jnp.float32)
    return out, carry + sums[:, keys:]


KEY_TILE = 256


def silu_product(gate, up):
    return (gate / (1.0 + jnp.exp(-gate)) * up).astype(jnp.bfloat16)


def program_kernel(
    groups,
    plane,
    query_ref,
    key_ref,
    value_ref,
    bias_ref,
    tri_ref,
    mixer_hbm,
    mixer_gain_ref,
    input_ref,
    entry_gain_ref,
    index_ref,
    weight_ref,
    exit_gain_ref,
    gate_hbm,
    up_hbm,
    down_hbm,
    shared_gate_hbm,
    shared_up_hbm,
    shared_down_hbm,
    mixer_out,
    expert_out,
    normed,
    outgoing,
    back,
    stage,
    rows,
    partial,
    first_sum,
    second_sum,
    result,
    returned,
    neighbours,
    shared_part,
    shared_first,
    shared_second,
    kv_own,
    query_own,
    kv_all,
    queries,
    running,
    carried,
    far_part,
    attended_back,
    attended,
    mixer_part,
    mixer_first,
    mixer_second,
    mixer_w,
    gate_w,
    up_w,
    down_w,
    shared_gate_w,
    shared_up_w,
    shared_down_w,
    mixing_high,
    mixing_low,
    shared_total,
    weight_sem,
    own_sem,
    z_send,
    z_recv,
    p_send,
    p_recv,
    x_send,
    x_recv,
    q_send,
    q_recv,
    b_send,
    b_recv,
    s_send,
    s_recv,
    a_send,
    a_recv,
):
    f32, bf16 = jnp.float32, jnp.bfloat16
    own_ep = lax.axis_index("ep")
    own_x = lax.axis_index("tp")
    own_z = own_ep // plane
    own_p = own_ep % plane
    own_y = own_p // 2
    own_core = own_p % 2
    lines = plane // 2
    half = plane // 2
    right = (own_x + 1) % 4
    left = (own_x + 3) % 4
    opposite = (own_x + 2) % 4
    side = (right, left)
    experts, width = gate_w.shape[0], gate_w.shape[1]
    shared_rows = normed.shape[0]
    shared_half = shared_rows // 2
    tokens = key_ref.shape[0]
    head_size = query_ref.shape[1] // lines
    mixer_rows = tokens // 4
    mixer_half = mixer_rows // 2
    slots = groups * plane * experts * CAPACITY

    def remote(src, dst, send_sem, recv_sem, ep, tp):
        return pltpu.make_async_remote_copy(
            src_ref=src,
            dst_ref=dst,
            send_sem=send_sem,
            recv_sem=recv_sem,
            device_id=(ep, tp),
            device_id_type=pl.DeviceIdType.MESH,
        )

    def offset(c):
        odd = c % 2
        return (odd * ((c + 1) // 2) + (1 - odd) * (groups - c // 2)) % groups

    def z_copy(c):
        there = (own_z + offset(c)) % groups
        return remote(
            outgoing.at[there], stage.at[c], z_send.at[c], z_recv.at[c], there * plane + own_p, own_x
        )

    def p_copy(c, i):
        there = (own_p + i) % plane
        return remote(
            stage.at[c, there],
            rows.at[0, c, own_p],
            p_send.at[c, i],
            p_recv.at[c, i],
            own_z * plane + there,
            own_x,
        )

    def p_own(c):
        return pltpu.make_async_copy(stage.at[c, own_p], rows.at[0, c, own_p], own_sem.at[0, c])

    def x_copy(c, way):
        return remote(
            rows.at[0, c], rows.at[1 + way, c], x_send.at[0, way, c], x_recv.at[0, way, c], own_ep, side[way]
        )

    def f_copy(c, way):
        part = pl.ds(way * half, half)
        return remote(
            rows.at[1 + way, c, part],
            rows.at[3, c, part],
            x_send.at[1, way, c],
            x_recv.at[1, way, c],
            own_ep,
            side[way],
        )

    def r_copy(c, way):
        return remote(
            partial.at[3, c, pl.ds(way * half, half)],
            first_sum.at[way, c],
            x_send.at[2, way, c],
            x_recv.at[2, way, c],
            own_ep,
            side[way],
        )

    def t_copy(c, way):
        return remote(
            partial.at[2 - way, c],
            second_sum.at[way, c],
            x_send.at[3, way, c],
            x_recv.at[3, way, c],
            own_ep,
            side[way],
        )

    def q_copy(c, i):
        there = (own_p + i) % plane
        return remote(
            result.at[c, there],
            returned.at[c, own_p],
            q_send.at[c, i],
            q_recv.at[c, i],
            own_z * plane + there,
            own_x,
        )

    def q_own(c):
        return pltpu.make_async_copy(result.at[c, own_p], returned.at[c, own_p], own_sem.at[1, c])

    def b_copy(c):
        there = (own_z + groups - offset(c)) % groups
        return remote(
            returned.at[c], back.at[own_z], b_send.at[c], b_recv.at[c], there * plane + own_p, own_x
        )

    def shared_copy(kind, way):
        part = pl.ds(way * shared_half, shared_half)
        src, dst = (
            (normed, neighbours.at[way]),
            (neighbours.at[way, part], neighbours.at[2, part]),
            (shared_part.at[3, part], shared_first.at[way]),
            (shared_part.at[2 - way], shared_second.at[way]),
        )[kind]
        return remote(src, dst, s_send.at[kind, way], s_recv.at[kind, way], own_ep, side[way])

    mirror = (groups - 1 - own_z) * plane + own_p
    partner = own_z * plane + own_p + 1 - 2 * own_core

    def k_copy(i):
        line = (own_y + i) % lines
        return remote(
            kv_own.at[line],
            kv_all.at[own_z, own_core, own_y],
            a_send.at[0, i],
            a_recv.at[0, i],
            own_z * plane + 2 * line + own_core,
            own_x,
        )

    def ask_copy(i):
        line = (own_y + i) % lines
        return remote(
            query_own.at[line],
            queries.at[own_y],
            a_send.at[1, i],
            a_recv.at[1, i],
            own_z * plane + 2 * line + own_core,
            own_x,
        )

    def kz_copy(c):
        there = (own_z + offset(c)) % groups
        block = kv_all.at[own_z, own_core]
        return remote(block, block, a_send.at[2, c], a_recv.at[2, c], there * plane + own_p, own_x)

    def kd_copy(c):
        source = (own_z + groups - offset(c)) % groups
        block = kv_all.at[source, own_core]
        return remote(block, block, a_send.at[3, c], a_recv.at[3, c], partner, own_x)

    def answer_copy(i):
        line = (own_y + i) % lines
        return remote(
            attended_back.at[line],
            attended.at[own_y],
            a_send.at[4, i],
            a_recv.at[4, i],
            own_z * plane + 2 * line + own_core,
            own_x,
        )

    ask_far = remote(
        queries.at[pl.ds(2, 2)], queries.at[pl.ds(4, 2)], a_send.at[5, 0], a_recv.at[5, 0], mirror, own_x
    )
    answer_far = remote(
        far_part, attended_back.at[pl.ds(2, 2)], a_send.at[5, 1], a_recv.at[5, 1], mirror, own_x
    )
    k_own = pltpu.make_async_copy(
        kv_own.at[own_y], kv_all.at[own_z, own_core, own_y], own_sem.at[2, 2]
    )
    ask_own = pltpu.make_async_copy(query_own.at[own_y], queries.at[own_y], own_sem.at[2, 3])
    answer_own = pltpu.make_async_copy(
        attended_back.at[own_y], attended.at[own_y], own_sem.at[2, 4]
    )

    def mixer_copy(kind, way):
        part = pl.ds(way * mixer_half, mixer_half)
        src, dst = (
            (mixer_part.at[opposite, part], mixer_first.at[way]),
            (mixer_part.at[side[way]], mixer_second.at[way]),
        )[kind]
        return remote(src, dst, s_send.at[4 + kind, way], s_recv.at[4 + kind, way], own_ep, side[way])

    first_z = pltpu.make_async_copy(outgoing.at[own_z], stage.at[0], own_sem.at[2, 0])
    last_z = pltpu.make_async_copy(returned.at[0], back.at[own_z], own_sem.at[2, 1])
    loads = [
        pltpu.make_async_copy(src, dst, weight_sem.at[n])
        for n, (src, dst) in enumerate(
            (
                (shared_gate_hbm, shared_gate_w),
                (shared_up_hbm, shared_up_w),
                (shared_down_hbm, shared_down_w),
                (gate_hbm, gate_w),
                (up_hbm, up_w),
                (down_hbm, down_w),
                (mixer_hbm, mixer_w),
            )
        )
    ]

    barrier = pltpu.get_barrier_semaphore()

    def greet(ep, tp):
        pl.semaphore_signal(
            barrier, inc=1, device_id=(ep, tp), device_id_type=pl.DeviceIdType.MESH
        )

    for k in range(1, groups):
        greet(((own_z + k) % groups) * plane + own_p, own_x)
    for k in range(1, plane):
        greet(own_z * plane + (own_p + k) % plane, own_x)
    greet(own_ep, right)
    greet(own_ep, left)
    for load in loads:
        load.start()

    normed[...] = root_norm(input_ref[...].astype(f32), entry_gain_ref[...]).astype(bf16)

    lane = lax.broadcasted_iota(jnp.int32, (tokens, 128), 1)
    low = lane < head_size
    eye = (lax.broadcasted_iota(jnp.int32, (tokens, tokens), 0) == lax.broadcasted_iota(
        jnp.int32, (tokens, tokens), 1
    )).astype(bf16)
    bias_rows = lax.dot_general(
        bias_ref[...], eye, (((0,), (0,)), ((), ())), preferred_element_type=f32
    )
    for head in range(lines):
        column = (head // 2) * 128

        def placed(ref, upper):
            group = ref[:, column : column + 128].astype(f32)
            return group if head % 2 == upper else pltpu.roll(group, head_size, 1)

        kv_own[head, :tokens] = jnp.where(low, placed(key_ref, 0), placed(value_ref, 1)).astype(bf16)
        kv_own[head, tokens:] = jnp.broadcast_to(bias_rows[head : head + 1], (16, 128)).astype(bf16)
        query_own[head] = jnp.where(low, placed(query_ref, 0) * head_size**-0.5, 0.0).astype(bf16)

    expert_lane = lax.broadcasted_iota(jnp.int32, (shared_rows, slots // CAPACITY), 1)
    slot_lane = lax.broadcasted_iota(jnp.int32, (shared_rows, slots), 1)
    named = [(expert_lane == index_ref[:, k : k + 1]).astype(f32) for k in range(2)]
    earlier = (
        lax.broadcasted_iota(jnp.int32, (shared_rows, shared_rows), 1)
        < lax.broadcasted_iota(jnp.int32, (shared_rows, shared_rows), 0)
    ).astype(bf16)
    before = jnp.dot(earlier, (named[0] + named[1]).astype(bf16), preferred_element_type=f32)

    def placed_in(k):
        rank = jnp.sum(named[k] * before, axis=1, keepdims=True).astype(jnp.int32)
        return slot_lane == index_ref[:, k : k + 1] * CAPACITY + rank

    chosen = [placed_in(k) for k in range(2)]
    selector = (chosen[0] | chosen[1]).astype(f32).astype(bf16)
    mixing = jnp.where(chosen[0], weight_ref[:, 0:1], 0.0) + jnp.where(
        chosen[1], weight_ref[:, 1:2], 0.0
    )
    mixing_high[...] = mixing.astype(bf16)
    mixing_low[...] = (mixing - mixing.astype(bf16).astype(f32)).astype(bf16)
    outgoing[...] = (
        lax.dot_general(
            selector, normed[...], (((0,), (0,)), ((), ())), preferred_element_type=f32
        )
        .astype(bf16)
        .reshape(outgoing.shape)
    )
    running[...] = jnp.zeros_like(running)
    carried[...] = jnp.zeros_like(carried)
    first_z.start()
    k_own.start()
    ask_own.start()
    pl.semaphore_wait(barrier, groups + plane)

    for way in range(2):
        shared_copy(0, way).start()
    for c in range(1, min(groups, 5)):
        z_copy(c).start()
    for i in range(1, lines):
        k_copy(i).start()
        ask_copy(i).start()
    first_z.wait()

    def compute_shared():
        def one_block(source, target):
            block = source[...]
            gate = jnp.dot(block, shared_gate_w[...], preferred_element_type=f32)
            up = jnp.dot(block, shared_up_w[...], preferred_element_type=f32)
            hidden = silu_product(gate, up)
            target[...] = jnp.dot(hidden, shared_down_w[...], preferred_element_type=f32).astype(bf16)

        one_block(normed, shared_part.at[0])
        for j in range(3):
            one_block(neighbours.at[j], shared_part.at[j + 1])

    def compute_rows(c):
        count = 4 * plane * CAPACITY
        for e in range(experts):
            block = rows[:, c, :, e].reshape(count, width)
            gate = jnp.dot(block, gate_w[e], preferred_element_type=f32)
            up = jnp.dot(block, up_w[e], preferred_element_type=f32)
            hidden = silu_product(gate, up)
            product = jnp.dot(hidden, down_w[e], preferred_element_type=f32).astype(bf16)
            partial[:, c, :, e] = product.reshape(4, plane, CAPACITY, width)

    def flat(value):
        return value.reshape(-1, width).astype(f32)

    def add_first(c):
        for way in range(2):
            part = pl.ds(way * half, half)
            total = flat(partial[2 - way, c, part]) + flat(first_sum[way, c])
            partial[2 - way, c, part] = total.astype(bf16).reshape(half, experts, CAPACITY, width)

    def add_second(c):
        total = flat(partial[0, c]) + flat(second_sum[0, c]) + flat(second_sum[1, c])
        result[c] = total.astype(bf16).reshape(plane, experts, CAPACITY, width)

    first_turns = lines * own_z + 2
    turns = lines * (groups - 1) + 6
    share = (turns + 3) // 4

    def attend_turn(turn, unused):
        second = jnp.where(turn >= first_turns, 1, 0)
        query_z = own_z + second * (groups - 1 - 2 * own_z)
        tile = (1 - second) * (first_turns - 1 - turn) + second * (
            lines * query_z + 3 - (turn - first_turns)
        )
        tile_z = tile // lines
        tile_y = tile % lines
        limit = ((query_z * lines + 2 * second) * 2 + own_core) * tokens - tile * 2 * tokens
        row = lax.broadcasted_iota(jnp.int32, (2 * tokens, 2 * tokens), 0)
        column = lax.broadcasted_iota(jnp.int32, (2 * tokens, 2 * tokens), 1)
        mask = column - (row + (row // tokens) * tokens) < limit
        query = queries[pl.ds(4 * second, 2)].reshape(2 * tokens, 128)
        blocks = [kv_all[tile_z, core, tile_y] for core in range(2)]
        block = jnp.concatenate([b[:tokens] for b in blocks], axis=0)
        bias = jnp.concatenate([b[tokens:][:1] for b in blocks], axis=1).astype(f32)
        out, carry = stick_block(query, block, block, bias, carried[second], tri_ref[...], mask)
        running[second] = running[second] + out
        carried[second] = carry
        return unused

    def finish_attention():
        low2 = lax.broadcasted_iota(jnp.int32, (2 * tokens, 128), 1) < head_size
        even = own_y % 2 == 0
        for second, target in ((0, attended_back.at[pl.ds(0, 2)]), (1, far_part)):
            value = running[second]
            value = jnp.where(even, pltpu.roll(value, head_size, 1), value)
            target[...] = value.astype(bf16).reshape(2, tokens, 128)

    def mix():
        low1 = lax.broadcasted_iota(jnp.int32, (tokens, 128), 1) < head_size
        groups_of_two = [
            jnp.where(low1, attended[2 * n].astype(f32), attended[2 * n + 1].astype(f32)).astype(bf16)
            for n in range(lines // 2)
        ]
        gathered = jnp.concatenate(groups_of_two, axis=1)
        product = jnp.dot(gathered, mixer_w[...], preferred_element_type=f32).astype(bf16)
        mixer_part[...] = product.reshape(4, mixer_rows, width)

    def step(s, unused):
        @pl.when(s < groups)
        def _():
            @pl.when(s > 0)
            def _():
                z_copy(s).wait_recv()

            p_own(s).start()
            for i in range(1, plane):
                p_copy(s, i).start()

        @pl.when(s == 1)
        def _():
            for i in range(1, lines):
                k_copy(i).wait_recv()
            k_own.wait()
            for c in range(1, min(groups, 3)):
                kz_copy(c).start()
            for c in range(5, groups):
                z_copy(c).start()
            for c in range(3, groups):
                kz_copy(c).start()
            kd_copy(0).start()
            for i in range(1, lines):
                ask_copy(i).wait_recv()
            ask_own.wait()
            ask_far.start()

        @pl.when(s == 2)
        def _():
            for way in range(2):
                shared_copy(0, way).wait_recv()
                shared_copy(1, way).start()

        @pl.when((s >= 1) & (s < groups + 1))
        def _():
            c = s - 1
            for i in range(1, plane):
                p_copy(c, i).wait_recv()
            p_own(c).wait()
            for way in range(2):
                x_copy(c, way).start()

        @pl.when((s >= 2) & (s < groups + 2))
        def _():
            c = s - 2
            for way in range(2):
                x_copy(c, way).wait_recv()
                f_copy(c, way).start()

        @pl.when(s == 3)
        def _():
            for load in loads:
                load.wait()
            for way in range(2):
                shared_copy(1, way).wait_recv()
            compute_shared()

        @pl.when((s >= 3) & (s < groups + 3))
        def _():
            c = s - 3
            for way in range(2):
                f_copy(c, way).wait_recv()
            compute_rows(c)
            for way in range(2):
                r_copy(c, way).start()

        @pl.when(s == max(groups, 4))
        def _():
            for way in range(2):
                shared_copy(2, way).start()

        @pl.when((s >= 4) & (s < groups + 4))
        def _():
            c = s - 4
            for way in range(2):
                r_copy(c, way).wait_recv()
            add_first(c)
            for way in range(2):
                t_copy(c, way).start()

        @pl.when(s == max(groups, 4) + 1)
        def _():
            for way in range(2):
                shared_copy(2, way).wait_recv()
                part = pl.ds(way * shared_half, shared_half)
                shared_part[2 - way, part] = (
                    shared_part[2 - way, part].astype(f32) + shared_first[way].astype(f32)
                ).astype(bf16)
            for way in range(2):
                shared_copy(3, way).start()

        @pl.when((s >= 5) & (s < groups + 5))
        def _():
            c = s - 5
            for way in range(2):
                t_copy(c, way).wait_recv()
            add_second(c)
            q_own(c).start()
            for i in range(1, plane):
                q_copy(c, i).start()

        @pl.when((s >= 6) & (s < groups + 6))
        def _():
            c = s - 6
            for i in range(1, plane):
                q_copy(c, i).wait_recv()
            q_own(c).wait()

            @pl.when(c > 0)
            def _():
                b_copy(c).start()

            @pl.when(c == 0)
            def _():
                last_z.start()

        @pl.when((s >= 3) & (s < 7))
        def _():
            for n in range(2):
                c = 2 * (s - 3) + n

                @pl.when((c > 0) & (c < groups))
                def _():
                    kz_copy(c).wait_recv()
                    kd_copy(c).start()

        @pl.when(s == 7)
        def _():
            for c in range(groups):
                kd_copy(c).wait_recv()
            ask_far.wait_recv()

        @pl.when((s >= 7) & (s < 11))
        def _():
            first = (s - 7) * share
            lax.fori_loop(first, jnp.minimum(first + share, turns), attend_turn, 0)

        @pl.when(s == 10)
        def _():
            finish_attention()
            answer_far.start()

        @pl.when(s == 11)
        def _():
            answer_far.wait_recv()
            answer_own.start()
            for i in range(1, lines):
                answer_copy(i).start()

        @pl.when(s == 12)
        def _():
            for i in range(1, lines):
                answer_copy(i).wait_recv()
            answer_own.wait()
            mix()
            for way in range(2):
                mixer_copy(0, way).start()

        @pl.when(s == 13)
        def _():
            for way in range(2):
                mixer_copy(0, way).wait_recv()
                part = pl.ds(way * mixer_half, mixer_half)
                mixer_part[side[way], part] = (
                    mixer_part[side[way], part].astype(f32) + mixer_first[way].astype(f32)
                ).astype(bf16)
            for way in range(2):
                mixer_copy(1, way).start()

        return unused

    lax.fori_loop(0, max(groups + 6, 14), step, 0)

    for way in range(2):
        shared_copy(3, way).wait_recv()
    shared_sum = (
        shared_part[0].astype(f32) + shared_second[0].astype(f32) + shared_second[1].astype(f32)
    )
    shared_total[...] = shared_sum
    for way in range(2):
        mixer_copy(1, way).wait_recv()
    mixer_out[...] = root_norm(
        mixer_part[own_x].astype(f32) + mixer_second[0].astype(f32) + mixer_second[1].astype(f32),
        mixer_gain_ref[...],
    ).astype(bf16)

    def drain(c, unused):
        for i in range(1, plane):
            p_copy(c, i).wait_send()
            q_copy(c, i).wait_send()
        kd_copy(c).wait_send()
        for way in range(2):
            for copy in (x_copy, f_copy, r_copy, t_copy):
                copy(c, way).wait_send()

        @pl.when(c > 0)
        def _():
            z_copy(c).wait_send()
            b_copy(c).wait_send()
            kz_copy(c).wait_send()

        return unused

    for c in range(1, groups):
        b_copy(c).wait_recv()
    last_z.wait()
    rows_back = back[...].reshape(slots, width)
    combined = (
        jnp.dot(mixing_high[...], rows_back, preferred_element_type=f32)
        + jnp.dot(mixing_low[...], rows_back, preferred_element_type=f32)
        + shared_total[...]
    )
    expert_out[...] = root_norm(combined, exit_gain_ref[...]).astype(bf16)
    lax.fori_loop(0, groups, drain, 0)
    for kind in range(4):
        for way in range(2):
            shared_copy(kind, way).wait_send()
    for way in range(2):
        for kind in range(2):
            mixer_copy(kind, way).wait_send()
    for i in range(1, lines):
        k_copy(i).wait_send()
        ask_copy(i).wait_send()
        answer_copy(i).wait_send()
    ask_far.wait_send()
    answer_far.wait_send()


def on_device(
    query_rows,
    key_rows,
    value_rows,
    key_bias,
    mixer_weight,
    mixer_gain,
    routed_input,
    entry_gain,
    expert_index,
    route_weights,
    expert_gate,
    expert_up,
    expert_down,
    shared_gate,
    shared_up,
    shared_down,
    exit_gain,
):
    bf16, f32 = jnp.bfloat16, jnp.float32
    plane = PLANE
    groups = lax.axis_size("ep") // plane
    lines, half = plane // 2, plane // 2
    tokens = query_rows.shape[0]
    count, width = routed_input.shape
    experts = expert_gate.shape[0]
    block = (plane, experts, CAPACITY, width)
    row = jnp.arange(2 * tokens)
    later = (row[:, None] > row[None, :]).astype(bf16)
    tri = jnp.concatenate([later, jnp.ones((2 * tokens, 128), bf16)], axis=1)
    vmem = pl.BlockSpec(memory_space=pltpu.VMEM)
    hbm = pl.BlockSpec(memory_space=pl.ANY)
    weights = (expert_gate, expert_up, expert_down, shared_gate, shared_up, shared_down)
    dma = pltpu.SemaphoreType.DMA
    return pl.pallas_call(
        functools.partial(program_kernel, groups, plane),
        out_shape=(
            jax.ShapeDtypeStruct((tokens // 4, width), bf16),
            jax.ShapeDtypeStruct((count, width), bf16),
        ),
        in_specs=[vmem] * 5 + [hbm] + [vmem] * 6 + [hbm] * 6,
        out_specs=(vmem, vmem),
        scratch_shapes=[
            pltpu.VMEM((count, width), bf16),
            pltpu.VMEM((groups,) + block, bf16),
            pltpu.VMEM((groups,) + block, bf16),
            pltpu.VMEM((groups,) + block, bf16),
            pltpu.VMEM((4, groups) + block, bf16),
            pltpu.VMEM((4, groups) + block, bf16),
            pltpu.VMEM((2, groups, half) + block[1:], bf16),
            pltpu.VMEM((2, groups) + block, bf16),
            pltpu.VMEM((groups,) + block, bf16),
            pltpu.VMEM((groups,) + block, bf16),
            pltpu.VMEM((3, count, width), bf16),
            pltpu.VMEM((4, count, width), bf16),
            pltpu.VMEM((2, count // 2, width), bf16),
            pltpu.VMEM((2, count, width), bf16),
            pltpu.VMEM((lines, tokens + 16, 128), bf16),
            pltpu.VMEM((lines, tokens, 128), bf16),
            pltpu.VMEM((groups, 2, lines, tokens + 16, 128), bf16),
            pltpu.VMEM((6, tokens, 128), bf16),
            pltpu.VMEM((2, 2 * tokens, 128), f32),
            pltpu.VMEM((2, 2 * tokens, 128), f32),
            pltpu.VMEM((2, tokens, 128), bf16),
            pltpu.VMEM((lines, tokens, 128), bf16),
            pltpu.VMEM((lines, tokens, 128), bf16),
            pltpu.VMEM((4, tokens // 4, width), bf16),
            pltpu.VMEM((2, tokens // 8, width), bf16),
            pltpu.VMEM((2, tokens // 4, width), bf16),
            pltpu.VMEM(mixer_weight.shape, bf16),
        ]
        + [pltpu.VMEM(w.shape, bf16) for w in weights]
        + [
            pltpu.VMEM((count, groups * plane * experts * CAPACITY), bf16),
            pltpu.VMEM((count, groups * plane * experts * CAPACITY), bf16),
            pltpu.VMEM((count, width), f32),
            dma((7,)),
            dma((3, max(groups, 5))),
            dma((groups,)),
            dma((groups,)),
            dma((groups, plane)),
            dma((groups, plane)),
            dma((4, 2, groups)),
            dma((4, 2, groups)),
            dma((groups, plane)),
            dma((groups, plane)),
            dma((groups,)),
            dma((groups,)),
            dma((6, 2)),
            dma((6, 2)),
            dma((6, max(groups, 4))),
            dma((6, max(groups, 4))),
        ],
        compiler_params=pltpu.CompilerParams(
            collective_id=1, has_side_effects=True, vmem_limit_bytes=62 << 20
        ),
        name="program",
    )(
        query_rows,
        key_rows,
        value_rows,
        key_bias,
        tri,
        mixer_weight,
        mixer_gain.reshape(1, width),
        routed_input,
        entry_gain.reshape(1, width),
        expert_index,
        route_weights,
        exit_gain.reshape(1, width),
        *weights,
    )


def solution(mesh):
    in_specs = (
        P("ep", "tp"),
        P("ep", "tp"),
        P("ep", "tp"),
        P("ep", "tp"),
        P("tp", None),
        P(),
        P(("ep", "tp"), None),
        P(),
        P(("ep", "tp"), None),
        P(("ep", "tp"), None),
        P("ep", None, "tp"),
        P("ep", None, "tp"),
        P("ep", "tp", None),
        P(None, "tp"),
        P(None, "tp"),
        P("tp", None),
        P(),
    )
    out_specs = (P(("ep", "tp"), None), P(("ep", "tp"), None))
    return jax.shard_map(
        on_device, mesh=mesh, in_specs=in_specs, out_specs=out_specs, check_vma=False
    )
```

time: 230 us -> 145 us (0.63)
  the two profiles are of different devices: /device:TPU:248 before, /device:TPU:65 now
where the time goes in v3:
time: 145 us
  Pallas kernels  136 us (94%)
  local copies, waits for them, and re-layouts  7.52 us (5%)
    pallas_call x1, Pallas kernels, on_device(): pl.pallas_call(functools.partial(program_kernel, groups, plane), out_shap...  136 us
    unnamed x5, local copies, waits for them, and re-layouts  7.52 us

profile of v3, /device:TPU:65, one launch (start us, length us, event | category | flops | bytes accessed | tf_op | source)
XLA Modules:
  0.0 145.2 jit_solution(10182713238700255273)
XLA Ops:
  0.6 1.4 copy.19.bias_ref
  2.0 1.4 copy.20.index_ref
  3.4 1.4 copy.21.weight_ref
  4.8 0.7 pad_convert_fusion.tri_ref
  5.5 136.3 %program.1 = (bf16[32,2048]{1,0:T(8,128)(2,1)}, bf16[96,2048]{1,0:T(8,128)(2,1)}) custom-call(bf16[128,256]{1,0:T(8,128)(2,1)} %query_ref.1, bf16[128,256]{1,0:T(8,128)(2,1)} %key_ref.1, bf16[128,256]{1,0:T(8,128)(2,1)} %value_ref.1, bf16[128,4]{1,0:T(8,128)(2,1)} %copy.19.bias_ref, bf16[256,384]{1,0:T(8,128)(2,1)} %pad_convert_fusion.tri_ref, ...), custom_call_target="tpu_custom_call" | custom-call | tf_op jit(solution)/shard_map/program/pallas_call | solution.py:749
  141.8 1.6 %copy.24 = bf16[32,2048]{1,0:T(8,128)(2,1)} copy(bf16[32,2048]{1,0:T(8,128)(2,1)} %get-tuple-element.4) | data formatting | bytes 262144
  143.4 1.8 %copy.25 = bf16[96,2048]{1,0:T(8,128)(2,1)} copy(bf16[96,2048]{1,0:T(8,128)(2,1)} %get-tuple-element.5) | data formatting | bytes 786432
  (1 shorter events, 0.0 us)

commit v4 on v3

v4 whole, which is shorter than its diff:
```python
import functools

import jax
import jax.numpy as jnp
from jax import lax
from jax.experimental import pallas as pl
from jax.experimental.pallas import tpu as pltpu
from jax.sharding import PartitionSpec as P

EPS = 1e-06
PLANE = 8
CAPACITY = 2
NEAR = 1
RING_STEPS = (3, 5, 6, 7)


def root_norm(values, gain_row):
    return values * lax.rsqrt(jnp.mean(values * values, axis=-1, keepdims=True) + EPS) * gain_row


def stick_turn(query, blocks, biases, carry, tri, masks):
    keys = tri.shape[0]
    levels, weights = [], []
    for block, bias, mask in zip(blocks, biases, masks):
        score = (
            lax.dot_general(
                query, block, (((1,), (1,)), ((), ())), preferred_element_type=jnp.float32
            )
            + bias
        )
        fail = jnp.maximum(score, 0.0) + jnp.log(1.0 + jnp.exp(-jnp.abs(score)))
        counted = fail if mask is None else jnp.where(mask, fail, 0.0)
        sums = jnp.dot(counted.astype(jnp.bfloat16), tri, preferred_element_type=jnp.float32)
        total = jnp.broadcast_to(sums[:, 0:1] + counted[:, 0:1], carry.shape)
        levels.append(((score - fail) - sums, total))
    for (level, total), mask in zip(levels, masks):
        weight = jnp.exp(level - jnp.concatenate([carry] * (keys // carry.shape[1]), axis=1))
        if mask is not None:
            weight = jnp.where(mask, weight, 0.0)
        weights.append(weight.astype(jnp.bfloat16))
        carry = carry + total
    out = jnp.dot(
        jnp.concatenate(weights, axis=1),
        jnp.concatenate(blocks, axis=0),
        preferred_element_type=jnp.float32,
    )
    return out, carry


def silu_product(gate, up):
    return (gate / (1.0 + jnp.exp(-gate)) * up).astype(jnp.bfloat16)


def program_kernel(
    groups,
    plane,
    query_ref,
    key_ref,
    value_ref,
    bias_ref,
    mixer_hbm,
    mixer_gain_ref,
    input_ref,
    entry_gain_ref,
    index_ref,
    weight_ref,
    exit_gain_ref,
    gate_hbm,
    up_hbm,
    down_hbm,
    shared_gate_hbm,
    shared_up_hbm,
    shared_down_hbm,
    mixer_out,
    expert_out,
    normed,
    outgoing,
    back,
    stage,
    rows,
    partial,
    first_sum,
    second_sum,
    result,
    returned,
    neighbours,
    shared_part,
    shared_first,
    shared_second,
    kv_own,
    query_own,
    kv_all,
    queries,
    running,
    carried,
    far_part,
    attended_back,
    attended,
    mixer_part,
    mixer_first,
    mixer_second,
    mixer_w,
    gate_w,
    up_w,
    down_w,
    shared_gate_w,
    shared_up_w,
    shared_down_w,
    mixing_high,
    mixing_low,
    tri_ref,
    meta,
    near_out,
    near_stage,
    near_return,
    weight_sem,
    own_sem,
    z_send,
    z_recv,
    p_send,
    p_recv,
    x_send,
    x_recv,
    q_send,
    q_recv,
    b_send,
    b_recv,
    s_send,
    s_recv,
    a_send,
    a_recv,
    n_send,
    n_recv,
    m_send,
    m_recv,
):
    f32, bf16 = jnp.float32, jnp.bfloat16
    own_ep = lax.axis_index("ep")
    own_x = lax.axis_index("tp")
    own_z = own_ep // plane
    own_p = own_ep % plane
    own_y = own_p // 2
    own_core = own_p % 2
    lines = plane // 2
    half = plane // 2
    right = (own_x + 1) % 4
    left = (own_x + 3) % 4
    opposite = (own_x + 2) % 4
    side = (right, left)
    experts, width = gate_w.shape[0], gate_w.shape[1]
    shared_rows = normed.shape[0]
    shared_half = shared_rows // 2
    tokens = key_ref.shape[0]
    head_size = query_ref.shape[1] // lines
    mixer_rows = tokens // 4
    mixer_half = mixer_rows // 2
    block_slots = plane * experts * CAPACITY
    slots = groups * block_slots
    near = min(NEAR, groups)
    far = groups - near
    kept = 1
    summed = groups - kept

    def remote(src, dst, send_sem, recv_sem, ep, tp):
        return pltpu.make_async_remote_copy(
            src_ref=src,
            dst_ref=dst,
            send_sem=send_sem,
            recv_sem=recv_sem,
            device_id=(ep, tp),
            device_id_type=pl.DeviceIdType.MESH,
        )

    def offset(c):
        odd = c % 2
        return (odd * ((c + 1) // 2) + (1 - odd) * (groups - c // 2)) % groups

    def z_copy(c):
        there = (own_z + offset(c)) % groups
        return remote(
            outgoing.at[there], stage.at[c], z_send.at[0], z_recv.at[c], there * plane + own_p, own_x
        )

    def p_copy(c, i):
        there = (own_p + i) % plane
        return remote(
            stage.at[c, there],
            rows.at[0, c, own_p],
            p_send.at[0],
            p_recv.at[c],
            own_z * plane + there,
            own_x,
        )

    def p_own(c):
        return pltpu.make_async_copy(stage.at[c, own_p], rows.at[0, c, own_p], own_sem.at[c])

    def x_copy(c, way):
        return remote(
            rows.at[0, c], rows.at[1 + way, c], x_send.at[0], x_recv.at[0, c], own_ep, side[way]
        )

    def f_copy(c, way):
        part = pl.ds(way * half, half)
        return remote(
            rows.at[1 + way, c, part],
            rows.at[3, c, part],
            x_send.at[1],
            x_recv.at[1, c],
            own_ep,
            side[way],
        )

    def r_copy(c, way):
        return remote(
            partial.at[3, c, pl.ds(way * half, half)],
            first_sum.at[way, c],
            x_send.at[2],
            x_recv.at[2, c],
            own_ep,
            side[way],
        )

    def t_copy(c, way):
        return remote(
            partial.at[2 - way, c],
            second_sum.at[way, c],
            x_send.at[3],
            x_recv.at[3, c],
            own_ep,
            side[way],
        )

    def q_copy(c, i):
        there = (own_p + i) % plane
        return remote(
            result.at[c, there],
            returned.at[c, own_p],
            q_send.at[0],
            q_recv.at[c],
            own_z * plane + there,
            own_x,
        )

    def q_own(c):
        return pltpu.make_async_copy(result.at[c, own_p], returned.at[c, own_p], own_sem.at[groups + c])

    def b_copy(c):
        there = (own_z + groups - offset(c)) % groups
        return remote(
            returned.at[c], back.at[c - kept], b_send.at[0], b_recv.at[0], there * plane + own_p, own_x
        )

    def shared_copy(kind, way):
        part = pl.ds(way * shared_half, shared_half)
        src, dst = (
            (normed, neighbours.at[way]),
            (neighbours.at[way, part], neighbours.at[2, part]),
            (shared_part.at[3, part], shared_first.at[way]),
            (shared_part.at[2 - way], shared_second.at[way]),
        )[kind]
        return remote(src, dst, s_send.at[kind], s_recv.at[kind], own_ep, side[way])

    mirror = (groups - 1 - own_z) * plane + own_p
    partner = own_z * plane + own_p + 1 - 2 * own_core

    def k_copy(i):
        line = (own_y + i) % lines
        return remote(
            kv_own.at[line],
            kv_all.at[own_z, own_core, own_y],
            a_send.at[0],
            a_recv.at[0],
            own_z * plane + 2 * line + own_core,
            own_x,
        )

    def ask_copy(i):
        line = (own_y + i) % lines
        return remote(
            query_own.at[line],
            queries.at[own_y],
            a_send.at[1],
            a_recv.at[1],
            own_z * plane + 2 * line + own_core,
            own_x,
        )

    def ring_copy(way, r):
        source = (own_z + groups + (2 * way - 1) * r) % groups
        there = (own_z + groups + 1 - 2 * way) % groups
        block = kv_all.at[source, own_core]
        return remote(
            block, block, a_send.at[6], a_recv.at[6 + way * hops[0] + r], there * plane + own_p, own_x
        )

    def core_copy(way, r):
        source = (own_z + groups + (2 * way - 1) * (r + 1)) % groups
        block = kv_all.at[source, own_core]
        return remote(block, block, a_send.at[3], a_recv.at[3], partner, own_x)

    def core_own():
        block = kv_all.at[own_z, own_core]
        return remote(block, block, a_send.at[3], a_recv.at[3], partner, own_x)

    hops = ((groups - 1) // 2, groups // 2)
    others = pl.ds(0, plane - 1)
    outer = pl.ds(0, lines - 1)

    def meter(ref, send_sem, recv_sem):
        return remote(ref, ref, send_sem, recv_sem, own_ep, right)

    def arrived(ref, sem):
        meter(ref, sem, sem).wait_recv()

    def left_here(ref, sem):
        meter(ref, sem, sem).wait_send()

    shared_landing = (
        neighbours.at[pl.ds(0, 2)],
        neighbours.at[2],
        shared_first,
        shared_second,
        mixer_first,
        mixer_second,
    )

    def shared_arrived(kind):
        arrived(shared_landing[kind], s_recv.at[kind])

    def x_arrived(kind, c):
        landing = (
            rows.at[pl.ds(1, 2), c],
            rows.at[3, c],
            first_sum.at[:, c],
            second_sum.at[:, c],
        )[kind]
        arrived(landing, x_recv.at[kind, c])

    def p_arrived(c):
        arrived(rows.at[0, c, others], p_recv.at[c])
        p_own(c).wait()

    def near_arrived(c):
        arrived(rows.at[pl.ds(1, 3), c, others], n_recv.at[3 + c])
        near_p_own(c).wait()

    def q_arrived(c):
        arrived(returned.at[c, others], q_recv.at[c])
        q_own(c).wait()


    def meta_copy(way):
        return remote(
            meta.at[0], meta.at[1 + way], m_send.at[0], m_recv.at[0], own_ep, side[way]
        )

    meta_far = remote(meta.at[1], meta.at[3], m_send.at[0], m_recv.at[1], own_ep, right)

    def near_z(c):
        there = (own_z + offset(c)) % groups
        return remote(
            near_out.at[c],
            near_stage.at[c - 1],
            n_send.at[0],
            n_recv.at[c],
            there * plane + own_p,
            own_x,
        )

    def near_source(c, place):
        return near_out.at[0, place] if c == 0 else near_stage.at[c - 1, place]

    def near_p(c, i):
        there = (own_p + i) % plane
        return remote(
            near_source(c, there),
            rows.at[pl.ds(1, 3), c, own_p],
            n_send.at[1],
            n_recv.at[3 + c],
            own_z * plane + there,
            own_x,
        )

    def near_p_own(c):
        return pltpu.make_async_copy(
            near_source(c, own_p), rows.at[pl.ds(1, 3), c, own_p], own_sem.at[2 * groups + 4 + c]
        )

    def near_q(c, i):
        there = (own_p + i) % plane
        return remote(
            partial.at[:, c, there],
            near_return.at[c, own_p],
            n_send.at[2],
            n_recv.at[6],
            own_z * plane + there,
            own_x,
        )

    def near_q_own(c):
        return pltpu.make_async_copy(
            partial.at[:, c, own_p], near_return.at[c, own_p], own_sem.at[2 * groups + 7]
        )

    def answer_copy(i):
        line = (own_y + i) % lines
        return remote(
            attended_back.at[line],
            attended.at[own_y],
            a_send.at[2],
            a_recv.at[2],
            own_z * plane + 2 * line + own_core,
            own_x,
        )

    ask_far = remote(
        queries.at[pl.ds(2, 2)], queries.at[pl.ds(4, 2)], a_send.at[4], a_recv.at[4], mirror, own_x
    )
    answer_far = remote(
        far_part, attended_back.at[pl.ds(2, 2)], a_send.at[5], a_recv.at[5], mirror, own_x
    )
    k_own = pltpu.make_async_copy(
        kv_own.at[own_y], kv_all.at[own_z, own_core, own_y], own_sem.at[2 * groups + 1]
    )
    ask_own = pltpu.make_async_copy(query_own.at[own_y], queries.at[own_y], own_sem.at[2 * groups + 2])
    answer_own = pltpu.make_async_copy(
        attended_back.at[own_y], attended.at[own_y], own_sem.at[2 * groups + 3]
    )

    def mixer_copy(kind, way):
        part = pl.ds(way * mixer_half, mixer_half)
        src, dst = (
            (mixer_part.at[opposite, part], mixer_first.at[way]),
            (mixer_part.at[side[way]], mixer_second.at[way]),
        )[kind]
        return remote(src, dst, s_send.at[4 + kind], s_recv.at[4 + kind], own_ep, side[way])

    first_z = pltpu.make_async_copy(outgoing.at[own_z], stage.at[0], own_sem.at[2 * groups])
    loads = [
        pltpu.make_async_copy(src, dst, weight_sem.at[n])
        for n, (src, dst) in enumerate(
            (
                (shared_gate_hbm, shared_gate_w),
                (shared_up_hbm, shared_up_w),
                (shared_down_hbm, shared_down_w),
                (gate_hbm, gate_w),
                (up_hbm, up_w),
                (down_hbm, down_w),
                (mixer_hbm, mixer_w),
            )
        )
    ]

    barrier = pltpu.get_barrier_semaphore()

    def greet(ep, tp):
        pl.semaphore_signal(
            barrier, inc=1, device_id=(ep, tp), device_id_type=pl.DeviceIdType.MESH
        )

    for k in range(1, groups):
        greet(((own_z + k) % groups) * plane + own_p, own_x)
    for k in range(1, plane):
        greet(own_z * plane + (own_p + k) % plane, own_x)
    greet(own_ep, right)
    greet(own_ep, left)
    for load in loads:
        load.start()

    normed[...] = root_norm(input_ref[...].astype(f32), entry_gain_ref[...]).astype(bf16)

    lane = lax.broadcasted_iota(jnp.int32, (tokens, 128), 1)
    low = lane < head_size
    bias_rows = bias_ref[...].astype(f32)
    tri_row = lax.broadcasted_iota(jnp.int32, tri_ref.shape, 0)
    tri_column = lax.broadcasted_iota(jnp.int32, tri_ref.shape, 1)
    tri_ref[...] = jnp.where(tri_row > tri_column, 1.0, 0.0).astype(bf16)
    for head in range(lines):
        column = (head // 2) * 128

        def placed(ref, upper):
            group = ref[:, column : column + 128].astype(f32)
            return group if head % 2 == upper else pltpu.roll(group, head_size, 1)

        kv_own[head, :tokens] = jnp.where(low, placed(key_ref, 0), placed(value_ref, 1)).astype(bf16)
        kv_own[head, tokens:] = jnp.broadcast_to(bias_rows[head : head + 1], (16, 128)).astype(bf16)
        query_own[head] = jnp.where(low, placed(query_ref, 0) * head_size**-0.5, 0.0).astype(bf16)

    expert_row = lax.broadcasted_iota(jnp.int32, (slots // CAPACITY, shared_rows), 0)
    named = [(expert_row == index_ref[k : k + 1]).astype(f32) for k in range(2)]
    earlier = (
        lax.broadcasted_iota(jnp.int32, (shared_rows, shared_rows), 0)
        < lax.broadcasted_iota(jnp.int32, (shared_rows, shared_rows), 1)
    ).astype(f32).astype(bf16)
    before = jnp.dot((named[0] + named[1]).astype(bf16), earlier, preferred_element_type=f32)
    meta[0] = jnp.zeros((8, 128), f32)
    for k in range(2):
        rank = jnp.sum(named[k] * before, axis=0, keepdims=True)
        meta[0, k : k + 1, :shared_rows] = index_ref[k : k + 1].astype(f32) * CAPACITY + rank
        meta[0, 2 + k : 3 + k, :shared_rows] = weight_ref[k : k + 1]

    def slot_hits(j, first, count):
        number = (lax.broadcasted_iota(jnp.int32, (count, shared_rows), 0) + first).astype(f32)
        return [number == meta[j, k : k + 1, :shared_rows] for k in range(2)]

    def picked(j, first, count):
        hits = slot_hits(j, first, count)
        return (hits[0] | hits[1]).astype(f32).astype(bf16)

    def weighted(j, first, count):
        hits = slot_hits(j, first, count)
        return jnp.where(hits[0], meta[j, 2:3, :shared_rows], 0.0) + jnp.where(
            hits[1], meta[j, 3:4, :shared_rows], 0.0
        )

    def chunk_first(c):
        return ((own_z + offset(c)) % groups) * block_slots

    def halves(value):
        high = value.astype(bf16)
        return high, (value - high.astype(f32)).astype(bf16)

    outgoing[...] = (
        jnp.dot(picked(0, 0, slots), normed[...], preferred_element_type=f32)
        .astype(bf16)
        .reshape(outgoing.shape)
    )
    for c in range(kept, groups):
        part = slice((c - kept) * block_slots, (c - kept + 1) * block_slots)
        mixing_high[part], mixing_low[part] = halves(weighted(0, chunk_first(c), block_slots))
    running[...] = jnp.zeros_like(running)
    carried[...] = jnp.zeros_like(carried)
    first_z.start()
    k_own.start()
    ask_own.start()
    pl.semaphore_wait(barrier, groups + plane)

    for way in range(2):
        shared_copy(0, way).start()
        meta_copy(way).start()
    for c in range(near, min(groups, near + 4)):
        z_copy(c).start()
    for i in range(1, lines):
        k_copy(i).start()
        ask_copy(i).start()
    first_z.wait()

    def compute_shared():
        def one_block(source, target):
            block = source[...]
            gate = jnp.dot(block, shared_gate_w[...], preferred_element_type=f32)
            up = jnp.dot(block, shared_up_w[...], preferred_element_type=f32)
            hidden = silu_product(gate, up)
            target[...] = jnp.dot(hidden, shared_down_w[...], preferred_element_type=f32).astype(bf16)

        one_block(normed, shared_part.at[0])
        for j in range(3):
            one_block(neighbours.at[j], shared_part.at[j + 1])

    def compute_rows(c):
        count = 4 * plane * CAPACITY
        for e in range(experts):
            block = rows[:, c, :, e].reshape(count, width)
            gate = jnp.dot(block, gate_w[e], preferred_element_type=f32)
            up = jnp.dot(block, up_w[e], preferred_element_type=f32)
            hidden = silu_product(gate, up)
            product = jnp.dot(hidden, down_w[e], preferred_element_type=f32).astype(bf16)
            partial[:, c, :, e] = product.reshape(4, plane, CAPACITY, width)

    def flat(value):
        return value.reshape(-1, width).astype(f32)

    def add_first(c):
        for way in range(2):
            part = pl.ds(way * half, half)
            total = flat(partial[2 - way, c, part]) + flat(first_sum[way, c])
            partial[2 - way, c, part] = total.astype(bf16).reshape(half, experts, CAPACITY, width)

    def add_second(c):
        total = flat(partial[0, c]) + flat(second_sum[0, c]) + flat(second_sum[1, c])
        result[c] = total.astype(bf16).reshape(plane, experts, CAPACITY, width)

    def gather_near():
        for j in range(1, 4):
            picks = jnp.concatenate([picked(j, chunk_first(c), block_slots) for c in range(near)], axis=0)
            chosen = jnp.dot(picks, neighbours[j - 1], preferred_element_type=f32).astype(bf16)
            near_out[:, :, j - 1] = chosen.reshape(near, plane, experts, CAPACITY, width)

    def combine_near():
        for j in range(4):
            mixing = weighted(j, chunk_first(0), block_slots)
            found = near_return[0, :, j].reshape(block_slots, width)
            total = shared_part[j].astype(f32)
            for piece in halves(mixing):
                total += lax.dot_general(
                    piece, found, (((0,), (0,)), ((), ())), preferred_element_type=f32
                )
            shared_part[j] = total.astype(bf16)

    first_turns = own_z + 1
    turns = groups + 1
    share = (turns + 2) // 3

    def attend_turn(turn, unused):
        second = jnp.where(turn >= first_turns, 1, 0)
        query_z = own_z + second * (groups - 1 - 2 * own_z)
        key_z = query_z - (turn - second * first_turns)

        def run(masked):
            query = queries[pl.ds(4 * second, 2)].reshape(2 * tokens, 128)
            blocks, biases, masks = [], [], []
            for line in range(lines - 1, -1, -1):
                pair = [kv_all[key_z, core, line] for core in range(2)]
                blocks.append(jnp.concatenate([b[:tokens] for b in pair], axis=0))
                biases.append(
                    jnp.concatenate([b[tokens:][:1] for b in pair], axis=1).astype(f32)
                )
                if masked:
                    row = lax.broadcasted_iota(jnp.int32, (2 * tokens, 2 * tokens), 0)
                    column = lax.broadcasted_iota(jnp.int32, (2 * tokens, 2 * tokens), 1)
                    limit = (2 * second - line) * 2 * tokens + own_core * tokens
                    masks.append(column - (row + (row // tokens) * tokens) < limit)
                else:
                    masks.append(None)
            out, carry = stick_turn(query, blocks, biases, carried[second], tri_ref[...], masks)
            running[second] = running[second] + out
            carried[second] = carry

        @pl.when(key_z == query_z)
        def _():
            run(True)

        @pl.when(key_z != query_z)
        def _():
            run(False)

        return unused

    def finish_attention():
        low2 = lax.broadcasted_iota(jnp.int32, (2 * tokens, 128), 1) < head_size
        even = own_y % 2 == 0
        for second, target in ((0, attended_back.at[pl.ds(0, 2)]), (1, far_part)):
            value = running[second]
            value = jnp.where(even, pltpu.roll(value, head_size, 1), value)
            target[...] = value.astype(bf16).reshape(2, tokens, 128)

    def mix():
        low1 = lax.broadcasted_iota(jnp.int32, (tokens, 128), 1) < head_size
        groups_of_two = [
            jnp.where(low1, attended[2 * n].astype(f32), attended[2 * n + 1].astype(f32)).astype(bf16)
            for n in range(lines // 2)
        ]
        gathered = jnp.concatenate(groups_of_two, axis=1)
        product = jnp.dot(gathered, mixer_w[...], preferred_element_type=f32).astype(bf16)
        mixer_part[...] = product.reshape(4, mixer_rows, width)

    def chunk(i):
        return i + near - (i // max(far, 1)) * summed

    def step(s, unused):
        @pl.when(s == 12)
        def _():
            answer_far.wait_recv()
            answer_own.start()
            for i in range(1, lines):
                answer_copy(i).start()

        @pl.when(s < far)
        def _():
            c = s + near
            z_copy(c).wait_recv()
            p_own(c).start()
            for i in range(1, plane):
                p_copy(c, i).start()

        @pl.when(s == 1)
        def _():
            arrived(kv_all.at[own_z, own_core, outer], a_recv.at[0])
            k_own.wait()
            for way in range(2):
                if hops[way] > 0:
                    ring_copy(way, 0).start()
            core_own().start()
            for c in range(near + 4, groups):
                z_copy(c).start()
            arrived(queries.at[outer], a_recv.at[1])
            ask_own.wait()
            ask_far.start()

        @pl.when(s == 2)
        def _():
            shared_arrived(0)
            arrived(meta.at[pl.ds(1, 2)], m_recv.at[0])
            for way in range(2):
                shared_copy(1, way).start()
            meta_far.start()

        @pl.when((s >= 1) & (s < far + 1))
        def _():
            c = s - 1 + near
            p_arrived(c)
            for way in range(2):
                x_copy(c, way).start()

        @pl.when((s >= 2) & (s < far + 2))
        def _():
            c = s - 2 + near
            x_arrived(0, c)
            for way in range(2):
                f_copy(c, way).start()

        for r in range(hops[1]):

            @pl.when(s == RING_STEPS[r])
            def _():
                for way in range(2):
                    if r < hops[way]:
                        ring_copy(way, r).wait_recv()
                        if r + 1 < hops[way]:
                            ring_copy(way, r + 1).start()
                        core_copy(way, r).start()

        @pl.when(s == 3)
        def _():
            shared_arrived(1)
            meta_far.wait_recv()
            gather_near()
            for c in range(1, near):
                near_z(c).start()
                z_copy(c).start()
            p_own(0).start()
            near_p_own(0).start()
            for i in range(1, plane):
                p_copy(0, i).start()
                near_p(0, i).start()

        @pl.when(s == 4)
        def _():
            for load in loads:
                load.wait()

        @pl.when((s >= 4) & (s < far + 4))
        def _():
            c = s - 4 + near
            x_arrived(1, c)
            compute_rows(c)
            for way in range(2):
                r_copy(c, way).start()

        @pl.when(s == 6)
        def _():
            p_arrived(0)
            near_arrived(0)
            compute_rows(0)
            near_q_own(0).start()
            for i in range(1, plane):
                near_q(0, i).start()

        for c in range(1, near):

            @pl.when(s == far + 3 + c)
            def _():
                p_arrived(c)
                near_arrived(c)
                compute_rows(c)
                for way in range(2):
                    r_copy(c, way).start()

        @pl.when((s >= 5) & (s < summed + 5))
        def _():
            c = chunk(s - 5)
            x_arrived(2, c)
            add_first(c)
            for way in range(2):
                t_copy(c, way).start()

        @pl.when((s >= 6) & (s < summed + 6))
        def _():
            c = chunk(s - 6)
            x_arrived(3, c)
            add_second(c)
            q_own(c).start()
            for i in range(1, plane):
                q_copy(c, i).start()

        @pl.when((s >= 8) & (s < summed + 8))
        def _():
            c = chunk(s - 8)
            q_arrived(c)
            b_copy(c).start()

        @pl.when(s == 5)
        def _():
            compute_shared()

        if near > 1:

            @pl.when(s == 7)
            def _():
                for c in range(1, near):
                    near_z(c).wait_recv()
                    z_copy(c).wait_recv()
                    p_own(c).start()
                    near_p_own(c).start()
                    for i in range(1, plane):
                        p_copy(c, i).start()
                        near_p(c, i).start()

        @pl.when(s == 8)
        def _():
            arrived(kv_all.at[:, 0], a_recv.at[3])
            ask_far.wait_recv()

        @pl.when((s >= 8) & (s < 11))
        def _():
            first = (s - 8) * share
            lax.fori_loop(first, jnp.minimum(first + share, turns), attend_turn, 0)

        @pl.when(s == 10)
        def _():
            finish_attention()
            answer_far.start()
            arrived(near_return.at[0, others], n_recv.at[6])
            near_q_own(0).wait()
            combine_near()

        @pl.when(s == 11)
        def _():
            for way in range(2):
                shared_copy(2, way).start()

        @pl.when(s == 12)
        def _():
            arrived(attended.at[outer], a_recv.at[2])
            answer_own.wait()
            mix()
            for way in range(2):
                mixer_copy(0, way).start()
            shared_arrived(2)
            for way in range(2):
                part = pl.ds(way * shared_half, shared_half)
                shared_part[2 - way, part] = (
                    shared_part[2 - way, part].astype(f32) + shared_first[way].astype(f32)
                ).astype(bf16)
                shared_copy(3, way).start()

        @pl.when(s == 13)
        def _():
            shared_arrived(4)
            for way in range(2):
                part = pl.ds(way * mixer_half, mixer_half)
                mixer_part[side[way], part] = (
                    mixer_part[side[way], part].astype(f32) + mixer_first[way].astype(f32)
                ).astype(bf16)
                mixer_copy(1, way).start()

        return unused

    lax.fori_loop(0, max(summed + 8, 14), step, 0)

    shared_arrived(5)
    mixer_out[...] = root_norm(
        mixer_part[own_x].astype(f32) + mixer_second[0].astype(f32) + mixer_second[1].astype(f32),
        mixer_gain_ref[...],
    ).astype(bf16)
    arrived(back, b_recv.at[0])
    rows_back = back[...].reshape(summed * block_slots, width)
    combined = sum(
        lax.dot_general(m[...], rows_back, (((0,), (0,)), ((), ())), preferred_element_type=f32)
        for m in (mixing_high, mixing_low)
    )
    shared_arrived(3)
    combined = (
        combined
        + shared_part[0].astype(f32)
        + shared_second[0].astype(f32)
        + shared_second[1].astype(f32)
    )
    expert_out[...] = root_norm(combined, exit_gain_ref[...]).astype(bf16)

    for ref, sem in (
        (stage.at[pl.ds(0, groups - 1)], z_send.at[0]),
        (stage.at[:, others], p_send.at[0]),
        (rows.at[pl.ds(0, 2), pl.ds(0, far)], x_send.at[0]),
        (rows.at[0, pl.ds(0, far)], x_send.at[1]),
        (partial.at[0, pl.ds(0, summed)], x_send.at[2]),
        (partial.at[pl.ds(0, 2), pl.ds(0, summed)], x_send.at[3]),
        (returned.at[pl.ds(0, summed), others], q_send.at[0]),
        (returned.at[pl.ds(0, summed)], b_send.at[0]),
        (meta.at[pl.ds(1, 3)], m_send.at[0]),
        (kv_all.at[own_z, own_core, outer], a_send.at[0]),
        (queries.at[outer], a_send.at[1]),
        (attended.at[outer], a_send.at[2]),
        (kv_all.at[:, 0], a_send.at[3]),
        (kv_all.at[pl.ds(0, groups - 1), 0], a_send.at[6]),
        (near_out.at[:, others], n_send.at[1]),
        (near_return.at[0, others], n_send.at[2]),
    ):
        left_here(ref, sem)
    if near > 1:
        left_here(near_stage.at[pl.ds(0, near - 1)], n_send.at[0])
    for kind, ref in enumerate(shared_landing):
        left_here(ref, s_send.at[kind])
    ask_far.wait_send()
    answer_far.wait_send()


def on_device(
    query_rows,
    key_rows,
    value_rows,
    key_bias,
    mixer_weight,
    mixer_gain,
    routed_input,
    entry_gain,
    expert_index,
    route_weights,
    expert_gate,
    expert_up,
    expert_down,
    shared_gate,
    shared_up,
    shared_down,
    exit_gain,
):
    bf16, f32 = jnp.bfloat16, jnp.float32
    plane = PLANE
    groups = lax.axis_size("ep") // plane
    lines, half = plane // 2, plane // 2
    tokens = query_rows.shape[0]
    count, width = routed_input.shape
    experts = expert_gate.shape[0]
    block = (plane, experts, CAPACITY, width)
    near = min(NEAR, groups)
    kept_slots = (groups - 1) * plane * experts * CAPACITY
    vmem = pl.BlockSpec(memory_space=pltpu.VMEM)
    hbm = pl.BlockSpec(memory_space=pl.ANY)
    weights = (expert_gate, expert_up, expert_down, shared_gate, shared_up, shared_down)
    dma = pltpu.SemaphoreType.DMA
    return pl.pallas_call(
        functools.partial(program_kernel, groups, plane),
        out_shape=(
            jax.ShapeDtypeStruct((tokens // 4, width), bf16),
            jax.ShapeDtypeStruct((count, width), bf16),
        ),
        in_specs=[vmem] * 4 + [hbm] + [vmem] * 6 + [hbm] * 6,
        out_specs=(vmem, vmem),
        scratch_shapes=[
            pltpu.VMEM((count, width), bf16),
            pltpu.VMEM((groups,) + block, bf16),
            pltpu.VMEM((groups - 1,) + block, bf16),
            pltpu.VMEM((groups,) + block, bf16),
            pltpu.VMEM((4, groups) + block, bf16),
            pltpu.VMEM((4, groups) + block, bf16),
            pltpu.VMEM((2, groups, half) + block[1:], bf16),
            pltpu.VMEM((2, groups) + block, bf16),
            pltpu.VMEM((groups,) + block, bf16),
            pltpu.VMEM((groups,) + block, bf16),
            pltpu.VMEM((3, count, width), bf16),
            pltpu.VMEM((4, count, width), bf16),
            pltpu.VMEM((2, count // 2, width), bf16),
            pltpu.VMEM((2, count, width), bf16),
            pltpu.VMEM((lines, tokens + 16, 128), bf16),
            pltpu.VMEM((lines, tokens, 128), bf16),
            pltpu.VMEM((groups, 2, lines, tokens + 16, 128), bf16),
            pltpu.VMEM((6, tokens, 128), bf16),
            pltpu.VMEM((2, 2 * tokens, 128), f32),
            pltpu.VMEM((2, 2 * tokens, 128), f32),
            pltpu.VMEM((2, tokens, 128), bf16),
            pltpu.VMEM((lines, tokens, 128), bf16),
            pltpu.VMEM((lines, tokens, 128), bf16),
            pltpu.VMEM((4, tokens // 4, width), bf16),
            pltpu.VMEM((2, tokens // 8, width), bf16),
            pltpu.VMEM((2, tokens // 4, width), bf16),
            pltpu.VMEM(mixer_weight.shape, bf16),
        ]
        + [pltpu.VMEM(w.shape, bf16) for w in weights]
        + [
            pltpu.VMEM((kept_slots, count), bf16),
            pltpu.VMEM((kept_slots, count), bf16),
            pltpu.VMEM((2 * tokens, 2 * tokens), bf16),
            pltpu.VMEM((4, 8, 128), f32),
            pltpu.VMEM((near, plane, 3) + block[1:], bf16),
            pltpu.VMEM((max(near - 1, 1), plane, 3) + block[1:], bf16),
            pltpu.VMEM((1, plane, 4) + block[1:], bf16),
            dma((7,)),
            dma((2 * groups + 8,)),
            dma((1,)),
            dma((groups,)),
            dma((1,)),
            dma((groups,)),
            dma((4,)),
            dma((4, groups)),
            dma((1,)),
            dma((groups,)),
            dma((1,)),
            dma((1,)),
            dma((6,)),
            dma((6,)),
            dma((7,)),
            dma((6 + groups,)),
            dma((3,)),
            dma((7,)),
            dma((1,)),
            dma((2,)),
        ],
        compiler_params=pltpu.CompilerParams(
            collective_id=1, has_side_effects=True, vmem_limit_bytes=62 << 20
        ),
        name="program",
    )(
        query_rows,
        key_rows,
        value_rows,
        jnp.transpose(key_bias),
        mixer_weight,
        mixer_gain.reshape(1, width),
        routed_input,
        entry_gain.reshape(1, width),
        jnp.transpose(expert_index),
        jnp.transpose(route_weights),
        exit_gain.reshape(1, width),
        *weights,
    )


def solution(mesh):
    in_specs = (
        P("ep", "tp"),
        P("ep", "tp"),
        P("ep", "tp"),
        P("ep", "tp"),
        P("tp", None),
        P(),
        P(("ep", "tp"), None),
        P(),
        P(("ep", "tp"), None),
        P(("ep", "tp"), None),
        P("ep", None, "tp"),
        P("ep", None, "tp"),
        P("ep", "tp", None),
        P(None, "tp"),
        P(None, "tp"),
        P("tp", None),
        P(),
    )
    out_specs = (P(("ep", "tp"), None), P(("ep", "tp"), None))
    return jax.shard_map(
        on_device, mesh=mesh, in_specs=in_specs, out_specs=out_specs, check_vma=False
    )
```

time: 145 us -> 119 us (0.82)
  the two profiles are of different devices: /device:TPU:65 before, /device:TPU:24 now
where the time goes in v4:
time: 119 us
  Pallas kernels  115 us (97%)
  local copies, waits for them, and re-layouts  3.33 us (3%)
    pallas_call x1, Pallas kernels, on_device(): pl.pallas_call(functools.partial(program_kernel, groups, plane), out_shap...  115 us
    unnamed x2, local copies, waits for them, and re-layouts  3.33 us

profile of v4, /device:TPU:24, one launch (start us, length us, event | category | flops | bytes accessed | tf_op | source)
XLA Modules:
  0.0 118.8 jit_solution(3102179912636986459)
XLA Ops:
  0.6 114.9 %program.1 = (bf16[32,2048]{1,0:T(8,128)(2,1)}, bf16[96,2048]{1,0:T(8,128)(2,1)}) custom-call(bf16[128,256]{1,0:T(8,128)(2,1)} %query_ref.1, bf16[128,256]{1,0:T(8,128)(2,1)} %key_ref.1, bf16[128,256]{1,0:T(8,128)(2,1)} %value_ref.1, bf16[4,128]{1,0:T(4,128)(2,1)} %bitcast.9, bf16[256,2048]{1,0:T(8,128)(2,1)} %mixer_hbm.1, f32[1,2048]{1,0:T(1,128)} %bitcast.6, ...), custom_call_target="tpu_custom_call" | custom-call | tf_op jit(solution)/shard_map/program/pallas_call | solution.py:942
  115.5 1.6 %copy.21 = bf16[32,2048]{1,0:T(8,128)(2,1)} copy(bf16[32,2048]{1,0:T(8,128)(2,1)} %get-tuple-element.4) | data formatting | bytes 262144
  117.1 1.8 %copy.22 = bf16[96,2048]{1,0:T(8,128)(2,1)} copy(bf16[96,2048]{1,0:T(8,128)(2,1)} %get-tuple-element.5) | data formatting | bytes 786432

commit v5 on v4

--- a/solution.py
+++ b/solution.py
@@ -10,7 +10,7 @@
 EPS = 1e-06
 PLANE = 8
 CAPACITY = 2
-NEAR = 1
+NEAR = 2
 RING_STEPS = (3, 5, 6, 7)
 
 
@@ -173,7 +173,7 @@
 
     def offset(c):
         odd = c % 2
-        return (odd * ((c + 1) // 2) + (1 - odd) * (groups - c // 2)) % groups
+        return (odd * (groups - (c + 1) // 2) + (1 - odd) * (c // 2)) % groups
 
     def z_copy(c):
         there = (own_z + offset(c)) % groups
@@ -659,13 +659,6 @@
         return i + near - (i // max(far, 1)) * summed
 
     def step(s, unused):
-        @pl.when(s == 12)
-        def _():
-            answer_far.wait_recv()
-            answer_own.start()
-            for i in range(1, lines):
-                answer_copy(i).start()
-
         @pl.when(s < far)
         def _():
             c = s + near
@@ -821,22 +814,17 @@
         def _():
             finish_attention()
             answer_far.start()
+
+        @pl.when(s == 10)
+        def _():
             arrived(near_return.at[0, others], n_recv.at[6])
             near_q_own(0).wait()
             combine_near()
-
-        @pl.when(s == 11)
-        def _():
             for way in range(2):
                 shared_copy(2, way).start()
 
-        @pl.when(s == 12)
-        def _():
-            arrived(attended.at[outer], a_recv.at[2])
-            answer_own.wait()
-            mix()
-            for way in range(2):
-                mixer_copy(0, way).start()
+        @pl.when(s == 11)
+        def _():
             shared_arrived(2)
             for way in range(2):
                 part = pl.ds(way * shared_half, shared_half)
@@ -845,25 +833,32 @@
                 ).astype(bf16)
                 shared_copy(3, way).start()
 
+        @pl.when(s == 12)
+        def _():
+            answer_far.wait_recv()
+            answer_own.start()
+            for i in range(1, lines):
+                answer_copy(i).start()
+
         @pl.when(s == 13)
         def _():
-            shared_arrived(4)
+            arrived(attended.at[outer], a_recv.at[2])
+            answer_own.wait()
+            mix()
             for way in range(2):
-                part = pl.ds(way * mixer_half, mixer_half)
-                mixer_part[side[way], part] = (
-                    mixer_part[side[way], part].astype(f32) + mixer_first[way].astype(f32)
-                ).astype(bf16)
-                mixer_copy(1, way).start()
+                mixer_copy(0, way).start()
 
         return unused
 
     lax.fori_loop(0, max(summed + 8, 14), step, 0)
 
-    shared_arrived(5)
-    mixer_out[...] = root_norm(
-        mixer_part[own_x].astype(f32) + mixer_second[0].astype(f32) + mixer_second[1].astype(f32),
-        mixer_gain_ref[...],
-    ).astype(bf16)
+    shared_arrived(4)
+    for way in range(2):
+        part = pl.ds(way * mixer_half, mixer_half)
+        mixer_part[side[way], part] = (
+            mixer_part[side[way], part].astype(f32) + mixer_first[way].astype(f32)
+        ).astype(bf16)
+        mixer_copy(1, way).start()
     arrived(back, b_recv.at[0])
     rows_back = back[...].reshape(summed * block_slots, width)
     combined = sum(
@@ -879,6 +874,11 @@
     )
     expert_out[...] = root_norm(combined, exit_gain_ref[...]).astype(bf16)
 
+    shared_arrived(5)
+    mixer_out[...] = root_norm(
+        mixer_part[own_x].astype(f32) + mixer_second[0].astype(f32) + mixer_second[1].astype(f32),
+        mixer_gain_ref[...],
+    ).astype(bf16)
     for ref, sem in (
         (stage.at[pl.ds(0, groups - 1)], z_send.at[0]),
         (stage.at[:, others], p_send.at[0]),

time: 119 us -> 115 us (0.966)
  the two profiles are of different devices: /device:TPU:24 before, /device:TPU:1 now
where the time goes in v5:
time: 115 us; the launch traced here: 114 us
  Pallas kernels  110 us (96%)
  local copies, waits for them, and re-layouts  3.33 us (3%)
    pallas_call x1, Pallas kernels, on_device(): pl.pallas_call(functools.partial(program_kernel, groups, plane), out_shap...  110 us
    unnamed x2, local copies, waits for them, and re-layouts  3.33 us

profile of v5, /device:TPU:1, one launch (start us, length us, event | category | flops | bytes accessed | tf_op | source)
XLA Modules:
  0.0 114.4 jit_solution(6861104674285090054)
XLA Ops:
  0.6 110.5 %program.1 = (bf16[32,2048]{1,0:T(8,128)(2,1)}, bf16[96,2048]{1,0:T(8,128)(2,1)}) custom-call(bf16[128,256]{1,0:T(8,128)(2,1)} %query_ref.1, bf16[128,256]{1,0:T(8,128)(2,1)} %key_ref.1, bf16[128,256]{1,0:T(8,128)(2,1)} %value_ref.1, bf16[4,128]{1,0:T(4,128)(2,1)} %bitcast.9, bf16[256,2048]{1,0:T(8,128)(2,1)} %mixer_hbm.1, f32[1,2048]{1,0:T(1,128)} %bitcast.6, ...), custom_call_target="tpu_custom_call" | custom-call | tf_op jit(solution)/shard_map/program/pallas_call | solution.py:942
  111.1 1.6 %copy.21 = bf16[32,2048]{1,0:T(8,128)(2,1)} copy(bf16[32,2048]{1,0:T(8,128)(2,1)} %get-tuple-element.4) | data formatting | bytes 262144
  112.7 1.8 %copy.22 = bf16[96,2048]{1,0:T(8,128)(2,1)} copy(bf16[96,2048]{1,0:T(8,128)(2,1)} %get-tuple-element.5) | data formatting | bytes 786432

commit v6 on v5

--- a/solution.py
+++ b/solution.py
@@ -815,7 +815,7 @@
             finish_attention()
             answer_far.start()
 
-        @pl.when(s == 10)
+        @pl.when(s == 9)
         def _():
             arrived(near_return.at[0, others], n_recv.at[6])
             near_q_own(0).wait()

time: 115 us -> 114 us (level)
  no operation moved by 1% of the time
where the time goes in v6:
time: 114 us
  Pallas kernels  110 us (96%)
  local copies, waits for them, and re-layouts  3.33 us (3%)
    pallas_call x1, Pallas kernels, on_device(): pl.pallas_call(functools.partial(program_kernel, groups, plane), out_shap...  110 us
    unnamed x2, local copies, waits for them, and re-layouts  3.33 us

profile of v6, /device:TPU:1, one launch (start us, length us, event | category | flops | bytes accessed | tf_op | source)
XLA Modules:
  0.0 114.2 jit_solution(10664108143127470073)
XLA Ops:
  0.6 110.2 %program.1 = (bf16[32,2048]{1,0:T(8,128)(2,1)}, bf16[96,2048]{1,0:T(8,128)(2,1)}) custom-call(bf16[128,256]{1,0:T(8,128)(2,1)} %query_ref.1, bf16[128,256]{1,0:T(8,128)(2,1)} %key_ref.1, bf16[128,256]{1,0:T(8,128)(2,1)} %value_ref.1, bf16[4,128]{1,0:T(4,128)(2,1)} %bitcast.9, bf16[256,2048]{1,0:T(8,128)(2,1)} %mixer_hbm.1, f32[1,2048]{1,0:T(1,128)} %bitcast.6, ...), custom_call_target="tpu_custom_call" | custom-call | tf_op jit(solution)/shard_map/program/pallas_call | solution.py:942
  110.9 1.6 %copy.21 = bf16[32,2048]{1,0:T(8,128)(2,1)} copy(bf16[32,2048]{1,0:T(8,128)(2,1)} %get-tuple-element.4) | data formatting | bytes 262144
  112.4 1.8 %copy.22 = bf16[96,2048]{1,0:T(8,128)(2,1)} copy(bf16[96,2048]{1,0:T(8,128)(2,1)} %get-tuple-element.5) | data formatting | bytes 786432
